TPU v7x, 32 devices: a whole 2x2x4 slice. The times are simulated.
32 devices in a mesh: sp: 16 (over z, y, core), tp: 2 (over x).
Axes of the slice: x: 2, y: 2, z: 4, core: 2. Of those that a mesh axis runs over, the one named last changes fastest.
Arguments:
- queries: bfloat16 [8192, 1024], P('sp', 'tp'), may hold values from -40 to 40
- keys_values: bfloat16 [8192, 4, 128], P('sp', 'tp'), may hold values from -40 to 40
- doc_ids: int32 [8192], P('sp'), may hold values from 0 to 3, never falling along the last dimension, each value on 1 to 4096 neighbouring positions
- head_sink: float32 [16], P('tp'), may hold values from 3 to 7
- out_weight: bfloat16 [1024, 2048], replicated, may hold values from -0.1875 to 0.1875
- hidden_in: bfloat16 [8192, 2048], P(('sp', 'tp')), may hold values from -0.59765625 to 0.59765625
- norm_gain: float32 [2048], replicated, may hold values from 0.1 to 1.9
- expert_gate: bfloat16 [32, 2048, 1024], P(('sp', 'tp')), may hold values from -0.125 to 0.125
- expert_up: bfloat16 [32, 2048, 1024], P(('sp', 'tp')), may hold values from -0.125 to 0.125
- expert_down: bfloat16 [32, 1024, 2048], P(('sp', 'tp')), may hold values from -0.1875 to 0.1875
- routes: int32 [8192, 2], P(('sp', 'tp')), may hold values from 0 to 31, all different within a row; in each aligned block of 256 rows (0 to 255, 256 to 511, ...) at most 32 rows name the same one
- route_weight: float32 [8192, 2], P(('sp', 'tp')), may hold values from 0.1 to 1
Outputs:
- layer_out: bfloat16 [8192, 2048], P(('sp', 'tp'))
Inputs may be any that keep to these rules, and one draw needn't show every extreme that they name: `routes`: in the rows of one device (aligned blocks of 256 tokens in order) no expert is named more than 32 times; some expert is named exactly 32 times in some blocks.
All inputs are finite; a program needn't handle non-finite values.
Results may differ from a plain program's by a relative error of at most 0.02.
Values may be sent and summed in bfloat16 or wider, within the bound.
A program may use at most 64 MiB of HBM per device.

v0:
```python
import functools

import jax
import jax.numpy as jnp
from jax import lax
from jax.experimental import pallas as pl
from jax.experimental.pallas import tpu as pltpu
from jax.sharding import PartitionSpec as P

HD = 64
WIN = 128
PLANES = 4
CUTS = 4
TILE = 256
MESH = pl.DeviceIdType.MESH


def with_halo(cells, axis, width):
    count = lax.axis_size(axis)
    ends = count - 1
    return jnp.concatenate(
        [
            lax.ppermute(cells[-width:], axis, [(i, (i + 1) % count) for i in range(ends)]),
            cells,
            lax.ppermute(cells[:width], axis, [((i + 1) % count, i) for i in range(ends)]),
        ],
        axis=0,
    )


def place(stride, tps):
    sp = lax.axis_index("sp")
    tp = lax.axis_index("tp")
    return lax.div(sp, stride), lax.rem(sp, stride), tp, lax.rem(sp, stride) * tps + tp


def greet(z, r, tp, p, planes, stride, tps):
    peers = stride * tps
    barrier = pltpu.get_barrier_semaphore()
    for k in range(1, peers):
        pd = lax.rem(p + k, peers)
        pl.semaphore_signal(
            barrier,
            inc=1,
            device_id=(z * stride + lax.div(pd, tps), lax.rem(pd, tps)),
            device_id_type=MESH,
        )

    @pl.when(z > 0)
    def _():
        pl.semaphore_signal(
            barrier, inc=1, device_id=((z - 1) * stride + r, tp), device_id_type=MESH
        )

    @pl.when(z < planes - 1)
    def _():
        pl.semaphore_signal(
            barrier, inc=1, device_id=((z + 1) * stride + r, tp), device_id_type=MESH
        )

    beside = (z > 0).astype(jnp.int32) + (z < planes - 1).astype(jnp.int32)
    pl.semaphore_wait(barrier, peers - 1 + beside)


def slot_hits(tab, z, slots, rows):
    ids = lax.broadcasted_iota(jnp.int32, (slots, rows), 0) + z * slots
    ids = ids.astype(jnp.float32)
    return ids == tab[0:1, :], ids == tab[1:2, :]


def dispatch_kernel(
    planes, stride, tps, cap,
    x_ref, tab_ref, gate_ref, up_ref, down_ref, out_ref, tab_out,
    toks, stage, zsend, zrecv, psend, precv, lsem,
    land, results, hidden, gate_w, up_w, down_w, tabs, tsend, trecv, wsem, ysem,
):
    z, r, tp, p = place(stride, tps)
    peers = stride * tps
    rows, width = x_ref.shape
    cols = width // CUTS
    slots = peers * cap
    greet(z, r, tp, p, planes, stride, tps)

    def span(h):
        return pl.ds(pl.multiple_of(h * cols, cols), cols)

    def hop(zs, h, side):
        return pltpu.make_async_remote_copy(
            src_ref=toks.at[zs, :, span(h)],
            dst_ref=toks.at[zs, :, span(h)],
            send_sem=zsend.at[side, zs, h],
            recv_sem=zrecv.at[zs, h],
            device_id=((z + 1 - 2 * side) * stride + r, tp),
            device_id_type=MESH,
        )

    def own_hop(h, side):
        return pltpu.make_async_remote_copy(
            src_ref=x_ref.at[:, span(h)],
            dst_ref=toks.at[z, :, span(h)],
            send_sem=zsend.at[side, z, h],
            recv_sem=zrecv.at[z, h],
            device_id=((z + 1 - 2 * side) * stride + r, tp),
            device_id_type=MESH,
        )

    def plane_copy(zs, h, dest, at):
        return pltpu.make_async_remote_copy(
            src_ref=stage.at[zs, pl.ds(pl.multiple_of(dest * cap, cap), cap), span(h)],
            dst_ref=land.at[zs, pl.ds(pl.multiple_of(at * cap, cap), cap), span(h)],
            send_sem=psend.at[zs, h, dest],
            recv_sem=precv.at[zs, h, at],
            device_id=(z * stride + lax.div(dest, tps), lax.rem(dest, tps)),
            device_id_type=MESH,
        )

    def local_copy(zs, h):
        return pltpu.make_async_copy(
            stage.at[zs, pl.ds(pl.multiple_of(p * cap, cap), cap), span(h)],
            land.at[zs, pl.ds(pl.multiple_of(p * cap, cap), cap), span(h)],
            lsem.at[zs, h],
        )

    def tab_hop(zs, side, source):
        return pltpu.make_async_remote_copy(
            src_ref=source,
            dst_ref=tabs.at[zs],
            send_sem=tsend.at[side, zs],
            recv_sem=trecv.at[zs],
            device_id=((z + 1 - 2 * side) * stride + r, tp),
            device_id_type=MESH,
        )

    loads = [
        pltpu.make_async_copy(source, target, wsem.at[k])
        for k, (source, target) in enumerate(
            [(gate_ref, gate_w), (up_ref, up_w), (down_ref, down_w)]
        )
    ]

    def result_copy(zs):
        return pltpu.make_async_copy(results.at[zs], out_ref.at[zs], ysem.at[zs])

    def experts(zs):
        @pl.loop(0, CUTS)
        def _(h):
            local_copy(zs, h).wait()
            for k in range(1, peers):
                other = lax.rem(p + k, peers)
                plane_copy(zs, h, other, other).wait_recv()

        @pl.loop(0, gate_w.shape[1] // TILE)
        def _(c):
            at = pl.ds(pl.multiple_of(c * TILE, TILE), TILE)
            gate = jnp.dot(land[zs], gate_w[:, at], preferred_element_type=jnp.float32)
            upper = jnp.dot(land[zs], up_w[:, at], preferred_element_type=jnp.float32)
            hidden[:, at] = (gate / (1.0 + jnp.exp(-gate)) * upper).astype(jnp.bfloat16)

        @pl.loop(0, width // TILE)
        def _(c):
            at = pl.ds(pl.multiple_of(c * TILE, TILE), TILE)
            results[zs, :, at] = jnp.dot(
                hidden[...], down_w[:, at], preferred_element_type=jnp.float32
            ).astype(jnp.bfloat16)

        result_copy(zs).start()

    def experts_at(dist):
        @pl.loop(0, 2)
        def _(side):
            zs = z - dist + 2 * dist * side

            @pl.when((zs >= 0) & (zs < planes) & ((dist > 0) | (side == 0)))
            def _():
                experts(zs)

    def pack(block, zs, h):
        first, second = slot_hits(tabs[zs], z, slots, rows)
        pick = jnp.where(first | second, 1.0, 0.0).astype(jnp.bfloat16)
        stage[zs, :, span(h)] = jnp.dot(
            pick, block, preferred_element_type=jnp.float32
        ).astype(jnp.bfloat16)
        for k in range(1, peers):
            plane_copy(zs, h, lax.rem(p + k, peers), p).start()
        local_copy(zs, h).start()

    @pl.when(z < planes - 1)
    def _():
        tab_hop(z, 0, tab_ref).start()

    @pl.when(z > 0)
    def _():
        tab_hop(z, 1, tab_ref).start()

    for h in range(CUTS):

        @pl.when(z < planes - 1)
        def _():
            own_hop(h, 0).start()

        @pl.when(z > 0)
        def _():
            own_hop(h, 1).start()

    for load in loads:
        load.start()
    tabs[z] = tab_ref[...]

    @pl.loop(0, CUTS)
    def _(h):
        pack(x_ref[:, span(h)], z, h)

    for load in loads:
        load.wait()

    @pl.loop(0, 2 * CUTS * (planes - 1))
    def _(e):
        dist = lax.div(e, 2 * CUTS) + 1
        h = lax.rem(lax.div(e, 2), CUTS)
        side = lax.rem(e, 2)
        zs = z - dist + 2 * dist * side

        @pl.when((zs >= 0) & (zs < planes))
        def _():
            onward = z + 1 - 2 * side

            @pl.when(h == 0)
            def _():
                tab_hop(zs, side, tabs.at[zs]).wait_recv()

                @pl.when((onward >= 0) & (onward < planes))
                def _():
                    tab_hop(zs, side, tabs.at[zs]).start()

            hop(zs, h, side).wait_recv()

            @pl.when((onward >= 0) & (onward < planes))
            def _():
                hop(zs, h, side).start()

            pack(toks[zs, :, span(h)], zs, h)

        @pl.when((side == 1) & (h == CUTS // 2 - 1))
        def _():
            experts_at(dist - 1)

    experts_at(planes - 1)

    @pl.loop(0, planes * CUTS)
    def _(e):
        zs = lax.div(e, CUTS)
        h = lax.rem(e, CUTS)

        @pl.when((zs <= z) & (z < planes - 1))
        def _():
            hop(zs, h, 0).wait_send()

        @pl.when((zs >= z) & (z > 0))
        def _():
            hop(zs, h, 1).wait_send()

        for k in range(1, peers):
            plane_copy(zs, h, lax.rem(p + k, peers), p).wait_send()

    @pl.loop(0, planes)
    def _(zs):
        @pl.when((zs <= z) & (z < planes - 1))
        def _():
            tab_hop(zs, 0, tabs.at[zs]).wait_send()

        @pl.when((zs >= z) & (z > 0))
        def _():
            tab_hop(zs, 1, tabs.at[zs]).wait_send()

        result_copy(zs).wait()

    tab_out[...] = tabs[...]


def return_kernel(
    planes, stride, tps, cap,
    y_ref, tab_ref, mid_ref, out_ref,
    held, part, from_low, from_high, zsend, lowrecv, highrecv, psend, precv, lsem, total,
):
    z, r, tp, p = place(stride, tps)
    peers = stride * tps
    rows, width = mid_ref.shape
    cols = width // CUTS
    slots = peers * cap
    greet(z, r, tp, p, planes, stride, tps)

    def span(h):
        return pl.ds(pl.multiple_of(h * cols, cols), cols)

    def plane_copy(zs, h, dest, at):
        return pltpu.make_async_remote_copy(
            src_ref=y_ref.at[zs, pl.ds(pl.multiple_of(dest * cap, cap), cap), span(h)],
            dst_ref=held.at[zs, pl.ds(pl.multiple_of(at * cap, cap), cap), span(h)],
            send_sem=psend.at[zs, h, dest],
            recv_sem=precv.at[zs, h, at],
            device_id=(z * stride + lax.div(dest, tps), lax.rem(dest, tps)),
            device_id_type=MESH,
        )

    def local_copy(zs, h):
        return pltpu.make_async_copy(
            y_ref.at[zs, pl.ds(pl.multiple_of(p * cap, cap), cap), span(h)],
            held.at[zs, pl.ds(pl.multiple_of(p * cap, cap), cap), span(h)],
            lsem.at[zs, h],
        )

    def send_out(zs, h):
        for k in range(1, peers):
            plane_copy(zs, h, lax.rem(p + k, peers), p).start()
        local_copy(zs, h).start()

    def up(zs, h):
        return pltpu.make_async_remote_copy(
            src_ref=part.at[zs, :, span(h)],
            dst_ref=from_low.at[zs, :, span(h)],
            send_sem=zsend.at[zs, h],
            recv_sem=lowrecv.at[zs, h],
            device_id=((z + 1) * stride + r, tp),
            device_id_type=MESH,
        )

    def down(zs, h):
        return pltpu.make_async_remote_copy(
            src_ref=part.at[zs, :, span(h)],
            dst_ref=from_high.at[zs, :, span(h)],
            send_sem=zsend.at[zs, h],
            recv_sem=highrecv.at[zs, h],
            device_id=((z - 1) * stride + r, tp),
            device_id_type=MESH,
        )

    def combined(zs, h):
        local_copy(zs, h).wait()
        for k in range(1, peers):
            plane_copy(zs, h, p, lax.rem(p + k, peers)).wait_recv()
        tab = tab_ref[zs]
        first, second = slot_hits(tab, z, slots, rows)
        mix = jnp.where(first, tab[2:3, :], 0.0) + jnp.where(second, tab[3:4, :], 0.0)
        return jnp.dot(
            mix.T.astype(jnp.bfloat16), held[zs, :, span(h)], preferred_element_type=jnp.float32
        )

    events = 2 * CUTS * (planes - 1)

    def event(e):
        dist = planes - 1 - lax.div(e, 2 * CUTS)
        h = lax.rem(lax.div(e, 2), CUTS)
        side = lax.rem(e, 2)
        zs = z + dist - 2 * dist * side
        return zs, h, side

    @pl.loop(0, events)
    def _(e):
        zs, h, side = event(e)

        @pl.when((zs >= 0) & (zs < planes))
        def _():
            send_out(zs, h)

    @pl.loop(0, CUTS)
    def _(h):
        send_out(z, h)

    @pl.loop(0, events)
    def _(e):
        zs, h, side = event(e)

        @pl.when((zs >= 0) & (zs < planes))
        def _():
            mine = combined(zs, h)
            part[zs, :, span(h)] = mine.astype(jnp.bfloat16)

            @pl.when((side == 0) & (z > 0))
            def _():
                up(zs, h).wait_recv()
                part[zs, :, span(h)] = (
                    part[zs, :, span(h)].astype(jnp.float32)
                    + from_low[zs, :, span(h)].astype(jnp.float32)
                ).astype(jnp.bfloat16)

            @pl.when((side == 1) & (z < planes - 1))
            def _():
                down(zs, h).wait_recv()
                part[zs, :, span(h)] = (
                    part[zs, :, span(h)].astype(jnp.float32)
                    + from_high[zs, :, span(h)].astype(jnp.float32)
                ).astype(jnp.bfloat16)

            @pl.when(side == 0)
            def _():
                up(zs, h).start()

            @pl.when(side == 1)
            def _():
                down(zs, h).start()

    @pl.loop(0, CUTS)
    def _(h):
        total[:, span(h)] = mid_ref[:, span(h)].astype(jnp.float32) + combined(z, h)

        @pl.when(z > 0)
        def _():
            up(z, h).wait_recv()
            total[:, span(h)] += from_low[z, :, span(h)].astype(jnp.float32)

        @pl.when(z < planes - 1)
        def _():
            down(z, h).wait_recv()
            total[:, span(h)] += from_high[z, :, span(h)].astype(jnp.float32)

        out_ref[:, span(h)] = total[:, span(h)].astype(jnp.bfloat16)

    @pl.loop(0, planes * CUTS)
    def _(e):
        zs = lax.div(e, CUTS)
        h = lax.rem(e, CUTS)

        @pl.when(zs > z)
        def _():
            up(zs, h).wait_send()

        @pl.when(zs < z)
        def _():
            down(zs, h).wait_send()

        for k in range(1, peers):
            plane_copy(zs, h, lax.rem(p + k, peers), p).wait_send()


def routed_by_plane(normed, mid, tab, planes, cap, weights):
    rows, width = normed.shape
    tps = lax.axis_size("tp")
    stride = lax.axis_size("sp") // planes
    peers = stride * tps
    dma = pltpu.SemaphoreType.DMA
    vmem = pl.BlockSpec(memory_space=pltpu.VMEM)
    anywhere = pl.BlockSpec(memory_space=pl.ANY)
    hidden = weights[0].shape[1]
    finished, tables = pl.pallas_call(
        functools.partial(dispatch_kernel, planes, stride, tps, cap),
        out_shape=[
            jax.ShapeDtypeStruct((planes, peers * cap, width), jnp.bfloat16),
            jax.ShapeDtypeStruct((planes,) + tab.shape, jnp.float32),
        ],
        in_specs=[vmem, vmem, anywhere, anywhere, anywhere],
        out_specs=[anywhere, vmem],
        scratch_shapes=[
            pltpu.VMEM((planes, rows, width), jnp.bfloat16),
            pltpu.VMEM((planes, peers * cap, width), jnp.bfloat16),
            dma((2, planes, CUTS)),
            dma((planes, CUTS)),
            dma((planes, CUTS, peers)),
            dma((planes, CUTS, peers)),
            dma((planes, CUTS)),
            pltpu.VMEM((planes, peers * cap, width), jnp.bfloat16),
            pltpu.VMEM((planes, peers * cap, width), jnp.bfloat16),
            pltpu.VMEM((peers * cap, hidden), jnp.bfloat16),
            pltpu.VMEM((width, hidden), jnp.bfloat16),
            pltpu.VMEM((width, hidden), jnp.bfloat16),
            pltpu.VMEM((hidden, width), jnp.bfloat16),
            pltpu.VMEM((planes,) + tab.shape, jnp.float32),
            dma((2, planes)),
            dma((planes,)),
            dma((3,)),
            dma((planes,)),
        ],
        compiler_params=pltpu.CompilerParams(
            collective_id=0, has_side_effects=True, vmem_limit_bytes=48 * 1024 * 1024
        ),
        name="dispatch",
    )(normed, tab, *weights)
    return pl.pallas_call(
        functools.partial(return_kernel, planes, stride, tps, cap),
        out_shape=jax.ShapeDtypeStruct((rows, width), jnp.bfloat16),
        in_specs=[anywhere, vmem, vmem],
        out_specs=vmem,
        scratch_shapes=[
            pltpu.VMEM((planes, peers * cap, width), jnp.bfloat16),
            pltpu.VMEM((planes, rows, width), jnp.bfloat16),
            pltpu.VMEM((planes, rows, width), jnp.bfloat16),
            pltpu.VMEM((planes, rows, width), jnp.bfloat16),
            dma((planes, CUTS)),
            dma((planes, CUTS)),
            dma((planes, CUTS)),
            dma((planes, CUTS, peers)),
            dma((planes, CUTS, peers)),
            dma((planes, CUTS)),
            pltpu.VMEM((rows, width), jnp.float32),
        ],
        compiler_params=pltpu.CompilerParams(
            collective_id=1, has_side_effects=True, vmem_limit_bytes=40 * 1024 * 1024
        ),
        name="combine",
    )(finished, tables, mid)


def expert_rows(arrived, gate_w, up_w, down_w):
    width = arrived.shape[-1]
    flat_rows = arrived.reshape(-1, width)
    gate = jnp.dot(flat_rows, gate_w, preferred_element_type=jnp.float32)
    upper = jnp.dot(flat_rows, up_w, preferred_element_type=jnp.float32)
    expert_hidden = (jax.nn.silu(gate) * upper).astype(jnp.bfloat16)
    result = jnp.dot(expert_hidden, down_w, preferred_element_type=jnp.float32).astype(jnp.bfloat16)
    return result.reshape(arrived.shape[:-1] + (result.shape[-1],))


def shards(
    queries,
    keys_values,
    doc_ids,
    head_sink,
    out_weight,
    hidden_in,
    norm_gain,
    expert_gate,
    expert_up,
    expert_down,
    routes,
    route_weight,
):
    tok_here = queries.shape[0]
    heads_here = head_sink.shape[0]
    kv_here = keys_values.shape[1]
    group = heads_here // kv_here
    head_dim = keys_values.shape[2] // 2
    docs_wide = jnp.broadcast_to(
        doc_ids.astype(jnp.bfloat16)[:, None], (tok_here, keys_values.shape[2])
    )
    slab = jnp.concatenate([keys_values.reshape(tok_here, -1), docs_wide], axis=1)
    slab = with_halo(slab, "sp", WIN)
    kv_ext = slab[:, : kv_here * keys_values.shape[2]].reshape(
        -1, kv_here, keys_values.shape[2]
    )
    docs_ext = slab[:, kv_here * keys_values.shape[2]].astype(jnp.int32)
    offset = lax.axis_index("sp") * tok_here
    seq_total = lax.axis_size("sp") * tok_here
    span_rows = min(512, tok_here)
    sink_logit = head_sink.reshape(kv_here, group)[:, :, None, None]

    def one_span(span_index):
        first_row = span_index * span_rows
        q_span = queries.reshape(span_rows, kv_here, group, head_dim)
        scores = jnp.einsum(
            "qhgd,khd->hgqk", q_span, kv_ext[..., :head_dim], preferred_element_type=jnp.float32
        ) * HD ** (-0.5)
        query_pos = offset + first_row + jnp.arange(span_rows, dtype=jnp.int32)
        key_pos = offset + first_row - WIN + jnp.arange(span_rows + 2 * WIN, dtype=jnp.int32)
        inside = (key_pos >= 0) & (key_pos < seq_total)
        allowed = (
            (jnp.abs(key_pos[None, :] - query_pos[:, None]) <= WIN)
            & inside[None, :]
            & (docs_ext[None, :] == doc_ids[:, None])
        )
        masked = jnp.where(allowed, scores, -1e30)
        row_max = jnp.maximum(masked.max(-1, keepdims=True), sink_logit)
        exp_scores = jnp.where(allowed, jnp.exp(masked - row_max), 0.0)
        total_mass = exp_scores.sum(-1, keepdims=True) + jnp.exp(sink_logit - row_max)
        weights = (exp_scores / total_mass).astype(jnp.bfloat16)
        outcome = jnp.einsum(
            "hgqk,khd->qhgd", weights, kv_ext[..., head_dim:], preferred_element_type=jnp.float32
        )
        return outcome.astype(jnp.bfloat16).reshape(span_rows, heads_here * head_dim)

    attended = lax.map(one_span, jnp.arange(tok_here // span_rows, dtype=jnp.int32)).reshape(
        tok_here, -1
    )
    if lax.axis_size("tp") == 2:
        tp = lax.axis_index("tp")
        half = tok_here // 2
        mine = lax.dynamic_slice_in_dim(attended, tp * half, half, 0)
        other = lax.ppermute(
            lax.dynamic_slice_in_dim(attended, (1 - tp) * half, half, 0), "tp", [(0, 1), (1, 0)]
        )
        gathered = jnp.concatenate(
            [jnp.where(tp == 0, mine, other), jnp.where(tp == 0, other, mine)], axis=1
        )
    else:
        gathered = lax.all_to_all(attended, "tp", split_axis=0, concat_axis=1, tiled=True)
    projected = jnp.dot(gathered, out_weight, preferred_element_type=jnp.float32)
    mid_wide = (hidden_in.astype(jnp.float32) + projected).astype(jnp.bfloat16).astype(jnp.float32)
    normed = (
        mid_wide
        * lax.rsqrt(jnp.mean(mid_wide * mid_wide, axis=-1, keepdims=True) + 1e-06)
        * norm_gain
    ).astype(jnp.bfloat16)
    local_rows = normed.shape[0]
    topk = routes.shape[1]
    width = normed.shape[1]
    sp_count = lax.axis_size("sp")
    tp_count = lax.axis_size("tp")
    expert_count = sp_count * tp_count
    capacity = 2 * local_rows * topk // expert_count
    flat_routes = routes.reshape(-1)
    one_hot = (flat_routes[:, None] == jnp.arange(expert_count, dtype=jnp.int32)[None, :]).astype(
        jnp.int32
    )
    slot_rank = (jnp.cumsum(one_hot, axis=0) * one_hot).sum(-1) - 1
    slot_index = flat_routes * capacity + slot_rank
    if capacity % 16 == 0 and sp_count % PLANES == 0 and topk == 2:
        tab = jnp.concatenate(
            [
                slot_index.reshape(local_rows, topk).astype(jnp.float32).T,
                route_weight.T,
                jnp.zeros((4, local_rows), jnp.float32),
            ],
            axis=0,
        )
        return routed_by_plane(
            normed,
            mid_wide.astype(jnp.bfloat16),
            tab,
            PLANES,
            capacity,
            (expert_gate[0], expert_up[0], expert_down[0]),
        )
    repeated = jnp.repeat(normed, topk, axis=0)
    buffer_rows = (
        jnp.zeros((expert_count * capacity, width), jnp.bfloat16).at[slot_index].set(repeated)
    )
    sent = buffer_rows.reshape(expert_count, capacity, width)
    finished = expert_rows(
        lax.all_to_all(sent, ("sp", "tp"), split_axis=0, concat_axis=0, tiled=True),
        expert_gate[0],
        expert_up[0],
        expert_down[0],
    )
    returned = lax.all_to_all(finished, ("sp", "tp"), split_axis=0, concat_axis=0, tiled=True)
    returned = returned.reshape(expert_count * capacity, width)
    picked = returned[slot_index].astype(jnp.float32).reshape(local_rows, topk, width)
    mixture = jnp.sum(picked * route_weight[..., None], axis=1)
    return (mid_wide + mixture).astype(jnp.bfloat16)


def solution(mesh):
    placed = (
        P("sp", "tp"),
        P("sp", "tp", None),
        P("sp"),
        P("tp"),
        P(),
        P(("sp", "tp"), None),
        P(),
        P(("sp", "tp"), None, None),
        P(("sp", "tp"), None, None),
        P(("sp", "tp"), None, None),
        P(("sp", "tp"), None),
        P(("sp", "tp"), None),
    )
    return jax.shard_map(
        shards, mesh=mesh, in_specs=placed, out_specs=P(("sp", "tp"), None), check_vma=False
    )
```

profile of v0, /device:TPU:9, one launch (start us, length us, event | category | flops | bytes accessed | tf_op | source)
XLA Modules:
  0.0 203.2 jit_solution(16920553727962454942)
XLA Ops:
  0.0 0.0 copy-start.2
  0.0 1.1 copy.26
  1.1 0.7 convert_element_type.46
  1.9 3.7 %collective-permute-start = (bf16[128,384]{0,1:T(8,128)(2,1)S(1)}, bf16[128,384]{0,1:T(8,128)(2,1)S(1)}, u32[]{:S(2)}, u32[]{:S(2)}) collective-permute-start(bf16[128,384]{0,1:T(8,128)(2,1)S(1)} %get-tuple-element.34), channel_id=1, source_target_pairs={{0,2},{2,4},{4,6},{6,8},{8,10},{10,12},{12,14},{14,16},{16,18},{18... | collective-permute-start | bytes 294920 | tf_op jit(solution)/shard_map/ppermute | solution.py:23
  5.6 1.9 collective-permute-start.1
  7.5 0.8 copy.19
  8.3 0.1 eq.57
  8.5 0.1 eq.53
  8.6 1.3 copy.17
  9.9 0.7 max.22
  10.7 1.2 reduce-window.6
  11.8 0.2 slice_reduce_fusion
  12.1 0.1 fusion.15
  12.2 0.1 sub.66
  12.4 0.1 copy.22
  12.4 0.0 collective-permute-done
  12.5 0.0 collective-permute-done.1
  12.5 0.1 pad_maximum_fusion
  12.6 0.0 copy-done.2
  12.6 0.9 fusion.8
  13.5 2.1 %fusion = (f32[2,4,512]{2,1,0:T(4,128)S(1)}, f32[2,768,512,4]{2,1,3,0:T(8,128)S(1)}) fusion(pred[512,768]{0,1:T(8,128)(4,1)S(1)} %fusion.8, bf16[512,2,4,64]{0,3,2,1:T(8,128)(2,1)S(1)} %bitcast.60, bf16[768,2,128]{0,2,1:T(8,128)(2,1)S(1)} %bitcast.61), kind=kOutput, calls=%fused_computation.3 | convolution fusion | flops 412086272 | bytes 13713408 | tf_op jit(solution)/shard_map/while/body/eval_jaxpr/qhgd,khd->hgqk/dot_general | solution.py:548
  15.6 0.1 broadcast_maximum_fusion
  15.7 3.1 %fusion.1 = f32[2,4,512]{2,1,0:T(4,128)S(1)} fusion(f32[2,768,512,4]{2,1,3,0:T(8,128)S(1)} %get-tuple-element.38, f32[2,4,512]{2,1,0:T(4,128)S(1)} %broadcast_maximum_fusion, pred[512,768]{0,1:T(8,128)(4,1)S(1)} %fusion.8), kind=kLoop, calls=%fused_computation.4 | loop fusion | flops 15724544 | bytes 13008896 | tf_op jit(solution)/shard_map/while/body/eval_jaxpr/reduce_sum | solution.py:562
  18.8 0.1 exponential_add_fusion
  18.8 0.0 copy-start.1
  18.9 0.0 copy-start.3
  18.9 0.0 copy-start.4
  18.9 4.0 %fusion.9 = bf16[2,64,4,512]{3,1,2,0:T(8,128)(2,1)S(1)} fusion(f32[2,768,512,4]{2,1,3,0:T(8,128)S(1)} %get-tuple-element.38, f32[2,4,512]{2,1,0:T(4,128)S(1)} %exponential_add_fusion, f32[2,4,512]{2,1,0:T(4,128)S(1)} %broadcast_maximum_fusion, pred[512,768]{0,1:T(8,128)(4,1)S(1)} %fusion.8, bf16[768,2,128]{0,2,1:T(8,128)(2,1)S(1)} %bitcast.62), kind=kOutput, calls=%fused_computation.16 | convolution fusion | flops 421789696 | bytes 13729792 | tf_op jit(solution)/shard_map/while/body/eval_jaxpr/hgqk,khd->qhgd/dot_general | solution.py:564
  22.9 1.3 collective-permute-start.2
  24.2 0.0 copy-done.1
  24.2 0.1 pad.2.clone
  24.3 0.0 copy-done.3
  24.3 0.1 maximum_maximum_fusion.tab_ref
  24.3 5.0 %collective-permute-done.2 = bf16[256,512]{0,1:T(8,128)(2,1)S(1)} collective-permute-done((bf16[256,512]{0,1:T(8,128)(2,1)S(1)}, bf16[256,512]{0,1:T(8,128)(2,1)S(1)}, u32[]{:S(2)}, u32[]{:S(2)}) %collective-permute-start.2) | collective-permute-done | bytes 262176 | tf_op jit(solution)/shard_map/ppermute | solution.py:576
  29.3 0.1 broadcast_select_fusion.1
  29.5 0.0 copy-done.4
  29.5 0.0 copy-start
  29.5 3.6 %fusion.4 = (f32[256]{0:T(256)S(1)}, bf16[256,2048]{1,0:T(8,128)(2,1)S(1)}) fusion(bf16[1024,2048]{1,0:T(8,128)(2,1)} %param.16, bf16[256,512]{0,1:T(8,128)(2,1)S(1)} %get-tuple-element.32, bf16[256,512]{0,1:T(8,128)(2,1)S(1)} %get-tuple-element.23, bf16[256,2048]{1,0:T(8,128)(2,1)S(1)} %copy-done.4), kind=kOutput, calls=%fused_computation.10 | convolution fusion | flops 1077935872 | bytes 6816768 | tf_op jit(solution)/shard_map/dot_general | solution.py:584
  33.1 0.0 copy-done
  33.1 0.3 fusion.6.x_ref
  33.5 75.5 %dispatch.1 = (bf16[4,256,2048]{2,1,0:T(8,128)(2,1)S(1)}, f32[4,8,256]{2,1,0:T(8,128)S(1)}) custom-call(bf16[256,2048]{1,0:T(8,128)(2,1)S(1)} %fusion.6.x_ref, f32[8,256]{1,0:T(8,128)S(1)} %maximum_maximum_fusion.tab_ref, bf16[2048,1024]{1,0:T(8,128)(2,1)} %bitcast.54, bf16[2048,1024]{1,0:T(8,128)(2,1)} %bitcast.55, bf16[1024,2048]{1,0:T(8,128)(2,1)} %bitcast.56), custom_call_target="tpu_custom_call" | custom-call | tf_op jit(solution)/shard_map/dispatch/pallas_call | solution.py:444
  109.0 93.3 %combine.1 = bf16[256,2048]{1,0:T(8,128)(2,1)S(1)} custom-call(bf16[4,256,2048]{2,1,0:T(8,128)(2,1)S(1)} %get-tuple-element.21.y_ref, f32[4,8,256]{2,1,0:T(8,128)S(1)} %get-tuple-element.22.tab_ref, bf16[256,2048]{1,0:T(8,128)(2,1)S(1)} %get-tuple-element.40.mid_ref), custom_call_target="tpu_custom_call" | custom-call | tf_op jit(solution)/shard_map/combine/pallas_call | solution.py:477
  202.3 1.0 copy.30
  (15 shorter events, 0.2 us)
Async XLA Ops:
  0.0 12.6 %copy-start.2 = (s32[512]{0:T(512)S(1)}, s32[512]{0:T(512)}, u32[]{:S(2)}) copy-start(s32[512]{0:T(512)} %param.14) | copy-start | bytes 6148
  1.9 10.6 %collective-permute-start = (bf16[128,384]{0,1:T(8,128)(2,1)S(1)}, bf16[128,384]{0,1:T(8,128)(2,1)S(1)}, u32[]{:S(2)}, u32[]{:S(2)}) collective-permute-start(bf16[128,384]{0,1:T(8,128)(2,1)S(1)} %get-tuple-element.34), channel_id=1, source_target_pairs={{0,2},{2,4},{4,6},{6,8},{8,10},{10,12},{12,14},{14,16},{16,18},{18... | collective-permute-start | bytes 294920 | tf_op jit(solution)/shard_map/ppermute | solution.py:23
  5.6 6.9 %collective-permute-start.1 = (bf16[128,384]{0,1:T(8,128)(2,1)S(1)}, bf16[128,384]{0,1:T(8,128)(2,1)S(1)}, u32[]{:S(2)}, u32[]{:S(2)}) collective-permute-start(bf16[128,384]{0,1:T(8,128)(2,1)S(1)} %get-tuple-element.36), channel_id=1, source_target_pairs={{2,0},{4,2},{6,4},{8,6},{10,8},{12,10},{14,12},{16,14},{18,16},{20... | collective-permute-start | bytes 294920 | tf_op jit(solution)/shard_map/ppermute | solution.py:25
  18.8 5.3 %copy-start.1 = (s32[256,2]{0,1:T(2,128)S(1)}, s32[256,2]{0,1:T(2,128)}, u32[]{:S(2)}) copy-start(s32[256,2]{0,1:T(2,128)} %param.22) | copy-start | bytes 6148
  18.9 5.4 %copy-start.3 = (f32[256,2]{0,1:T(2,128)S(1)}, f32[256,2]{0,1:T(2,128)}, u32[]{:S(2)}) copy-start(f32[256,2]{0,1:T(2,128)} %param.23) | copy-start | bytes 6148
  18.9 10.6 %copy-start.4 = (bf16[256,2048]{1,0:T(8,128)(2,1)S(1)}, bf16[256,2048]{1,0:T(8,128)(2,1)}, u32[]{:S(2)}) copy-start(bf16[256,2048]{1,0:T(8,128)(2,1)} %param.17) | copy-start | bytes 3145732
  22.9 6.4 %collective-permute-start.2 = (bf16[256,512]{0,1:T(8,128)(2,1)S(1)}, bf16[256,512]{0,1:T(8,128)(2,1)S(1)}, u32[]{:S(2)}, u32[]{:S(2)}) collective-permute-start(bf16[256,512]{0,1:T(8,128)(2,1)S(1)} %constant_dynamic-slice_fusion), channel_id=1, source_target_pairs={{0,1},{1,0},{2,3},{3,2},{4,5},{5,4},{6,7},{7,6},{8,9},{9,8},{10,11... | collective-permute-start | bytes 786440 | tf_op jit(solution)/shard_map/ppermute | solution.py:576
  29.5 3.6 %copy-start = (f32[2048]{0:T(1024)S(1)}, f32[2048]{0:T(1024)}, u32[]{:S(2)}) copy-start(f32[2048]{0:T(1024)} %param.18) | copy-start | bytes 24580
where the time goes:
time: 204 us; the launch traced here: 203 us
  Pallas kernels  169 us (83%)
  matrix products  9.7 us (5%)
  starting transfers between devices  6.9 us (3%)
  other arithmetic  6.79 us (3%)
  local copies, waits for them, and re-layouts  5.8 us (3%)
  waiting for transfers between devices  5.01 us (2%)
    pallas_call x1, Pallas kernels, routed_by_plane(): pl.pallas_call(functools.partial(return_kernel, planes, stride, tps, cap)...  93.3 us
    pallas_call x1, Pallas kernels, routed_by_plane(): pl.pallas_call(functools.partial(dispatch_kernel, planes, stride, tps, ca...  75.5 us
    ppermute x1, waiting for transfers between devices, shards(): lax.ppermute(lax.dynamic_slice_in_dim(attended, (1 - tp) * half, half, 0)...  5 us
  transfers between devices with their start and end apart: 3, of which 1 were waited for; matrix products, arithmetic and copies ran while one was open for 2% of the time, Pallas kernels for 0%

commit v1 on v0

v1 whole, which is shorter than its diff:
```python
import functools

import jax
import jax.numpy as jnp
from jax import lax
from jax.experimental import pallas as pl
from jax.experimental.pallas import tpu as pltpu
from jax.sharding import PartitionSpec as P

HD = 64
WIN = 128
PLANES = 4
CUTS = 4
TILE = 256
MESH = pl.DeviceIdType.MESH


def with_halo(cells, axis, width):
    count = lax.axis_size(axis)
    ends = count - 1
    return jnp.concatenate(
        [
            lax.ppermute(cells[-width:], axis, [(i, (i + 1) % count) for i in range(ends)]),
            cells,
            lax.ppermute(cells[:width], axis, [((i + 1) % count, i) for i in range(ends)]),
        ],
        axis=0,
    )


def place(stride, tps):
    sp = lax.axis_index("sp")
    tp = lax.axis_index("tp")
    return lax.div(sp, stride), lax.rem(sp, stride), tp, lax.rem(sp, stride) * tps + tp


def greet(z, r, tp, p, planes, stride, tps):
    peers = stride * tps
    barrier = pltpu.get_barrier_semaphore()
    for k in range(1, peers):
        pd = lax.rem(p + k, peers)
        pl.semaphore_signal(
            barrier,
            inc=1,
            device_id=(z * stride + lax.div(pd, tps), lax.rem(pd, tps)),
            device_id_type=MESH,
        )

    @pl.when(z > 0)
    def _():
        pl.semaphore_signal(
            barrier, inc=1, device_id=((z - 1) * stride + r, tp), device_id_type=MESH
        )

    @pl.when(z < planes - 1)
    def _():
        pl.semaphore_signal(
            barrier, inc=1, device_id=((z + 1) * stride + r, tp), device_id_type=MESH
        )

    beside = (z > 0).astype(jnp.int32) + (z < planes - 1).astype(jnp.int32)
    pl.semaphore_wait(barrier, peers - 1 + beside)


def slot_hits(tab, z, slots, rows):
    ids = lax.broadcasted_iota(jnp.int32, (slots, rows), 0) + z * slots
    ids = ids.astype(jnp.float32)
    return ids == tab[0:1, :], ids == tab[1:2, :]


def layer_kernel(
    planes, stride, tps, cap,
    x_ref, tab_ref, mid_ref, gate_ref, up_ref, down_ref, out_ref,
    toks, stage, land, results, held, part, from_low, from_high,
    gate_w, up_w, down_w, hidden, mixer, total, tabs,
    zsend, zrecv, psend, precv, rsend, rrecv, csend, lowrecv, highrecv, tsend, trecv, wsem,
):
    z, r, tp, p = place(stride, tps)
    peers = stride * tps
    rows, width = x_ref.shape
    cols = width // CUTS
    slots = peers * cap
    near = planes - 1
    greet(z, r, tp, p, planes, stride, tps)

    def span(h):
        return pl.ds(pl.multiple_of(h * cols, cols), cols)

    def seat(k):
        return pl.ds(pl.multiple_of(k * cap, cap), cap)

    def beside(side):
        return ((z + 1 - 2 * side) * stride + r, tp)

    def fellow(k):
        return (z * stride + lax.div(k, tps), lax.rem(k, tps))

    def hop(zs, h, side):
        return pltpu.make_async_remote_copy(
            src_ref=toks.at[zs, :, span(h)],
            dst_ref=toks.at[zs, :, span(h)],
            send_sem=zsend.at[side, zs, h],
            recv_sem=zrecv.at[zs, h],
            device_id=beside(side),
            device_id_type=MESH,
        )

    def own_hop(h, side):
        return pltpu.make_async_remote_copy(
            src_ref=x_ref.at[:, span(h)],
            dst_ref=toks.at[z, :, span(h)],
            send_sem=zsend.at[side, z, h],
            recv_sem=zrecv.at[z, h],
            device_id=beside(side),
            device_id_type=MESH,
        )

    def tab_hop(zs, side, source):
        return pltpu.make_async_remote_copy(
            src_ref=source,
            dst_ref=tabs.at[zs],
            send_sem=tsend.at[side, zs],
            recv_sem=trecv.at[zs],
            device_id=beside(side),
            device_id_type=MESH,
        )

    def give(zs, h, dest, at):
        return pltpu.make_async_remote_copy(
            src_ref=stage.at[zs, seat(dest), span(h)],
            dst_ref=land.at[zs, seat(at), span(h)],
            send_sem=psend.at[zs, h, dest],
            recv_sem=precv.at[zs, h, at],
            device_id=fellow(dest),
            device_id_type=MESH,
        )

    def back(zs, h, dest, at):
        return pltpu.make_async_remote_copy(
            src_ref=results.at[zs, seat(dest), span(h)],
            dst_ref=held.at[zs, seat(at), span(h)],
            send_sem=rsend.at[zs, h, dest],
            recv_sem=rrecv.at[zs, h, at],
            device_id=fellow(dest),
            device_id_type=MESH,
        )

    def climb(zs, h):
        return pltpu.make_async_remote_copy(
            src_ref=part.at[zs, :, span(h)],
            dst_ref=from_low.at[zs, :, span(h)],
            send_sem=csend.at[zs, h],
            recv_sem=lowrecv.at[zs, h],
            device_id=beside(0),
            device_id_type=MESH,
        )

    def sink(zs, h):
        return pltpu.make_async_remote_copy(
            src_ref=part.at[zs, :, span(h)],
            dst_ref=from_high.at[zs, :, span(h)],
            send_sem=csend.at[zs, h],
            recv_sem=highrecv.at[zs, h],
            device_id=beside(1),
            device_id_type=MESH,
        )

    loads = [
        pltpu.make_async_copy(source, target, wsem.at[k])
        for k, (source, target) in enumerate(
            [(gate_ref, gate_w), (up_ref, up_w), (down_ref, down_w)]
        )
    ]

    def pack(block, zs, h):
        first, second = slot_hits(tabs[zs], z, slots, rows)
        pick = jnp.where(first | second, 1.0, 0.0).astype(jnp.bfloat16)
        picked = jnp.dot(pick, block, preferred_element_type=jnp.float32)
        stage[zs, :, span(h)] = picked.astype(jnp.bfloat16)
        for k in range(1, peers):
            give(zs, h, lax.rem(p + k, peers), p).start()
        land[zs, seat(p), span(h)] = stage[zs, seat(p), span(h)]

    def experts(zs):
        tab = tabs[zs]
        first, second = slot_hits(tab, z, slots, rows)
        mix = jnp.where(first, tab[2:3, :], 0.0) + jnp.where(second, tab[3:4, :], 0.0)
        mixer[zs] = mix.T.astype(jnp.bfloat16)

        @pl.loop(0, CUTS)
        def _(h):
            for k in range(1, peers):
                other = lax.rem(p + k, peers)
                give(zs, h, other, other).wait_recv()

        @pl.loop(0, gate_w.shape[1] // TILE)
        def _(c):
            at = pl.ds(pl.multiple_of(c * TILE, TILE), TILE)
            gate = jnp.dot(land[zs], gate_w[:, at], preferred_element_type=jnp.float32)
            upper = jnp.dot(land[zs], up_w[:, at], preferred_element_type=jnp.float32)
            hidden[:, at] = (gate / (1.0 + jnp.exp(-gate)) * upper).astype(jnp.bfloat16)

        @pl.loop(0, CUTS)
        def _(h):
            @pl.loop(0, cols // TILE)
            def _(c):
                at = pl.ds(pl.multiple_of(h * cols + c * TILE, TILE), TILE)
                results[zs, :, at] = jnp.dot(
                    hidden[...], down_w[:, at], preferred_element_type=jnp.float32
                ).astype(jnp.bfloat16)

            for k in range(1, peers):
                back(zs, h, lax.rem(p + k, peers), p).start()
            held[zs, seat(p), span(h)] = results[zs, seat(p), span(h)]

    def mixed(zs, h):
        for k in range(1, peers):
            back(zs, h, p, lax.rem(p + k, peers)).wait_recv()
        return jnp.dot(mixer[zs], held[zs, :, span(h)], preferred_element_type=jnp.float32)

    def homeward(stage_of, h):
        @pl.loop(0, 2)
        def _(k):
            down = (k == 0) == (z >= planes // 2)
            zs = jnp.where(down, near - stage_of, stage_of)

            @pl.when(down & (zs < z))
            def _():
                part[zs, :, span(h)] = mixed(zs, h).astype(jnp.bfloat16)

                @pl.when(z < near)
                def _():
                    sink(zs, h).wait_recv()
                    part[zs, :, span(h)] += from_high[zs, :, span(h)]

                sink(zs, h).start()

            @pl.when(jnp.logical_not(down) & (zs > z))
            def _():
                part[zs, :, span(h)] = mixed(zs, h).astype(jnp.bfloat16)

                @pl.when(z > 0)
                def _():
                    climb(zs, h).wait_recv()
                    part[zs, :, span(h)] += from_low[zs, :, span(h)]

                climb(zs, h).start()

    @pl.when(z < near)
    def _():
        tab_hop(z, 0, tab_ref).start()

    @pl.when(z > 0)
    def _():
        tab_hop(z, 1, tab_ref).start()

    for h in range(CUTS):

        @pl.when(z < near)
        def _():
            own_hop(h, 0).start()

        @pl.when(z > 0)
        def _():
            own_hop(h, 1).start()

    for load in loads:
        load.start()
    tabs[z] = tab_ref[...]

    @pl.loop(0, CUTS)
    def _(h):
        pack(x_ref[:, span(h)], z, h)

    for load in loads:
        load.wait()

    @pl.loop(CUTS, (planes + 1) * CUTS)
    def _(e):
        dist = lax.div(e, CUTS)
        h = lax.rem(e, CUTS)

        @pl.loop(0, 2)
        def _(side):
            zs = z - dist + 2 * dist * side
            onward = z + 1 - 2 * side

            @pl.when((zs >= 0) & (zs < planes))
            def _():
                @pl.when(h == 0)
                def _():
                    tab_hop(zs, side, tabs.at[zs]).wait_recv()

                    @pl.when((onward >= 0) & (onward < planes))
                    def _():
                        tab_hop(zs, side, tabs.at[zs]).start()

                hop(zs, h, side).wait_recv()

                @pl.when((onward >= 0) & (onward < planes))
                def _():
                    hop(zs, h, side).start()

                pack(toks[zs, :, span(h)], zs, h)

        @pl.when(h == 0)
        def _():
            @pl.loop(0, 2)
            def _(side):
                zs = z - (dist - 1) + 2 * (dist - 1) * side

                @pl.when((zs >= 0) & (zs < planes) & ((dist > 1) | (side == 0)))
                def _():
                    experts(zs)

        @pl.when((dist > 1) & (h > 0))
        def _():
            homeward(dist - 1, h - 1)

        @pl.when((dist > 1) & (h == CUTS - 1))
        def _():
            homeward(dist - 1, h)

        @pl.when(dist == planes - 1)
        def _():
            total[:, span(h)] = mid_ref[:, span(h)].astype(jnp.float32) + mixed(z, h)

    @pl.loop(0, CUTS)
    def _(h):
        @pl.when(z > 0)
        def _():
            climb(z, h).wait_recv()
            total[:, span(h)] += from_low[z, :, span(h)].astype(jnp.float32)

        @pl.when(z < near)
        def _():
            sink(z, h).wait_recv()
            total[:, span(h)] += from_high[z, :, span(h)].astype(jnp.float32)

        out_ref[:, span(h)] = total[:, span(h)].astype(jnp.bfloat16)

    @pl.loop(0, planes * CUTS)
    def _(e):
        zs = lax.div(e, CUTS)
        h = lax.rem(e, CUTS)

        @pl.when((zs <= z) & (z < near))
        def _():
            hop(zs, h, 0).wait_send()

        @pl.when((zs >= z) & (z > 0))
        def _():
            hop(zs, h, 1).wait_send()

        @pl.when(zs > z)
        def _():
            climb(zs, h).wait_send()

        @pl.when(zs < z)
        def _():
            sink(zs, h).wait_send()

        for k in range(1, peers):
            give(zs, h, lax.rem(p + k, peers), p).wait_send()
            back(zs, h, lax.rem(p + k, peers), p).wait_send()

        @pl.when(h == 0)
        def _():
            @pl.when((zs <= z) & (z < near))
            def _():
                tab_hop(zs, 0, tabs.at[zs]).wait_send()

            @pl.when((zs >= z) & (z > 0))
            def _():
                tab_hop(zs, 1, tabs.at[zs]).wait_send()


def routed_by_plane(normed, mid, tab, planes, cap, weights):
    rows, width = normed.shape
    tps = lax.axis_size("tp")
    stride = lax.axis_size("sp") // planes
    peers = stride * tps
    slots = peers * cap
    dma = pltpu.SemaphoreType.DMA
    vmem = pl.BlockSpec(memory_space=pltpu.VMEM)
    anywhere = pl.BlockSpec(memory_space=pl.ANY)
    hidden = weights[0].shape[1]
    by_slot = pltpu.VMEM((planes, slots, width), jnp.bfloat16)
    by_row = pltpu.VMEM((planes, rows, width), jnp.bfloat16)
    chunks = dma((planes, CUTS))
    fans = dma((planes, CUTS, peers))
    return pl.pallas_call(
        functools.partial(layer_kernel, planes, stride, tps, cap),
        out_shape=jax.ShapeDtypeStruct((rows, width), jnp.bfloat16),
        in_specs=[vmem, vmem, vmem, anywhere, anywhere, anywhere],
        out_specs=vmem,
        scratch_shapes=[
            by_row, by_slot, by_slot, by_slot, by_slot, by_row, by_row, by_row,
            pltpu.VMEM((width, hidden), jnp.bfloat16),
            pltpu.VMEM((width, hidden), jnp.bfloat16),
            pltpu.VMEM((hidden, width), jnp.bfloat16),
            pltpu.VMEM((slots, hidden), jnp.bfloat16),
            pltpu.VMEM((planes, rows, slots), jnp.bfloat16),
            pltpu.VMEM((rows, width), jnp.float32),
            pltpu.VMEM((planes,) + tab.shape, jnp.float32),
            dma((2, planes, CUTS)), chunks, fans, fans, fans, fans, chunks, chunks, chunks,
            dma((2, planes)), dma((planes,)), dma((3,)),
        ],
        compiler_params=pltpu.CompilerParams(
            collective_id=0, has_side_effects=True, vmem_limit_bytes=60 * 1024 * 1024
        ),
        name="routed",
    )(normed, tab, mid, *weights)


def expert_rows(arrived, gate_w, up_w, down_w):
    width = arrived.shape[-1]
    flat_rows = arrived.reshape(-1, width)
    gate = jnp.dot(flat_rows, gate_w, preferred_element_type=jnp.float32)
    upper = jnp.dot(flat_rows, up_w, preferred_element_type=jnp.float32)
    expert_hidden = (jax.nn.silu(gate) * upper).astype(jnp.bfloat16)
    result = jnp.dot(expert_hidden, down_w, preferred_element_type=jnp.float32).astype(jnp.bfloat16)
    return result.reshape(arrived.shape[:-1] + (result.shape[-1],))


def shards(
    queries,
    keys_values,
    doc_ids,
    head_sink,
    out_weight,
    hidden_in,
    norm_gain,
    expert_gate,
    expert_up,
    expert_down,
    routes,
    route_weight,
):
    tok_here = queries.shape[0]
    heads_here = head_sink.shape[0]
    kv_here = keys_values.shape[1]
    group = heads_here // kv_here
    head_dim = keys_values.shape[2] // 2
    docs_wide = jnp.broadcast_to(
        doc_ids.astype(jnp.bfloat16)[:, None], (tok_here, keys_values.shape[2])
    )
    slab = jnp.concatenate([keys_values.reshape(tok_here, -1), docs_wide], axis=1)
    slab = with_halo(slab, "sp", WIN)
    kv_ext = slab[:, : kv_here * keys_values.shape[2]].reshape(
        -1, kv_here, keys_values.shape[2]
    )
    docs_ext = slab[:, kv_here * keys_values.shape[2]].astype(jnp.int32)
    offset = lax.axis_index("sp") * tok_here
    seq_total = lax.axis_size("sp") * tok_here
    span_rows = min(512, tok_here)
    sink_logit = head_sink.reshape(kv_here, group)[:, :, None, None]

    def one_span(span_index):
        first_row = span_index * span_rows
        q_span = queries.reshape(span_rows, kv_here, group, head_dim)
        scores = jnp.einsum(
            "qhgd,khd->hgqk", q_span, kv_ext[..., :head_dim], preferred_element_type=jnp.float32
        ) * HD ** (-0.5)
        query_pos = offset + first_row + jnp.arange(span_rows, dtype=jnp.int32)
        key_pos = offset + first_row - WIN + jnp.arange(span_rows + 2 * WIN, dtype=jnp.int32)
        inside = (key_pos >= 0) & (key_pos < seq_total)
        allowed = (
            (jnp.abs(key_pos[None, :] - query_pos[:, None]) <= WIN)
            & inside[None, :]
            & (docs_ext[None, :] == doc_ids[:, None])
        )
        masked = jnp.where(allowed, scores, -1e30)
        row_max = jnp.maximum(masked.max(-1, keepdims=True), sink_logit)
        exp_scores = jnp.where(allowed, jnp.exp(masked - row_max), 0.0)
        total_mass = exp_scores.sum(-1, keepdims=True) + jnp.exp(sink_logit - row_max)
        weights = (exp_scores / total_mass).astype(jnp.bfloat16)
        outcome = jnp.einsum(
            "hgqk,khd->qhgd", weights, kv_ext[..., head_dim:], preferred_element_type=jnp.float32
        )
        return outcome.astype(jnp.bfloat16).reshape(span_rows, heads_here * head_dim)

    attended = lax.map(one_span, jnp.arange(tok_here // span_rows, dtype=jnp.int32)).reshape(
        tok_here, -1
    )
    if lax.axis_size("tp") == 2:
        tp = lax.axis_index("tp")
        half = tok_here // 2
        mine = lax.dynamic_slice_in_dim(attended, tp * half, half, 0)
        other = lax.ppermute(
            lax.dynamic_slice_in_dim(attended, (1 - tp) * half, half, 0), "tp", [(0, 1), (1, 0)]
        )
        gathered = jnp.concatenate(
            [jnp.where(tp == 0, mine, other), jnp.where(tp == 0, other, mine)], axis=1
        )
    else:
        gathered = lax.all_to_all(attended, "tp", split_axis=0, concat_axis=1, tiled=True)
    projected = jnp.dot(gathered, out_weight, preferred_element_type=jnp.float32)
    mid_wide = (hidden_in.astype(jnp.float32) + projected).astype(jnp.bfloat16).astype(jnp.float32)
    normed = (
        mid_wide
        * lax.rsqrt(jnp.mean(mid_wide * mid_wide, axis=-1, keepdims=True) + 1e-06)
        * norm_gain
    ).astype(jnp.bfloat16)
    local_rows = normed.shape[0]
    topk = routes.shape[1]
    width = normed.shape[1]
    sp_count = lax.axis_size("sp")
    tp_count = lax.axis_size("tp")
    expert_count = sp_count * tp_count
    capacity = 2 * local_rows * topk // expert_count
    flat_routes = routes.reshape(-1)
    one_hot = (flat_routes[:, None] == jnp.arange(expert_count, dtype=jnp.int32)[None, :]).astype(
        jnp.int32
    )
    slot_rank = (jnp.cumsum(one_hot, axis=0) * one_hot).sum(-1) - 1
    slot_index = flat_routes * capacity + slot_rank
    if capacity % 16 == 0 and sp_count % PLANES == 0 and topk == 2:
        tab = jnp.concatenate(
            [
                slot_index.reshape(local_rows, topk).astype(jnp.float32).T,
                route_weight.T,
                jnp.zeros((4, local_rows), jnp.float32),
            ],
            axis=0,
        )
        return routed_by_plane(
            normed,
            mid_wide.astype(jnp.bfloat16),
            tab,
            PLANES,
            capacity,
            (expert_gate[0], expert_up[0], expert_down[0]),
        )
    repeated = jnp.repeat(normed, topk, axis=0)
    buffer_rows = (
        jnp.zeros((expert_count * capacity, width), jnp.bfloat16).at[slot_index].set(repeated)
    )
    sent = buffer_rows.reshape(expert_count, capacity, width)
    finished = expert_rows(
        lax.all_to_all(sent, ("sp", "tp"), split_axis=0, concat_axis=0, tiled=True),
        expert_gate[0],
        expert_up[0],
        expert_down[0],
    )
    returned = lax.all_to_all(finished, ("sp", "tp"), split_axis=0, concat_axis=0, tiled=True)
    returned = returned.reshape(expert_count * capacity, width)
    picked = returned[slot_index].astype(jnp.float32).reshape(local_rows, topk, width)
    mixture = jnp.sum(picked * route_weight[..., None], axis=1)
    return (mid_wide + mixture).astype(jnp.bfloat16)


def solution(mesh):
    placed = (
        P("sp", "tp"),
        P("sp", "tp", None),
        P("sp"),
        P("tp"),
        P(),
        P(("sp", "tp"), None),
        P(),
        P(("sp", "tp"), None, None),
        P(("sp", "tp"), None, None),
        P(("sp", "tp"), None, None),
        P(("sp", "tp"), None),
        P(("sp", "tp"), None),
    )
    return jax.shard_map(
        shards, mesh=mesh, in_specs=placed, out_specs=P(("sp", "tp"), None), check_vma=False
    )
```

time: 204 us -> 199 us (0.975)
  the two profiles are of different devices: /device:TPU:9 before, /device:TPU:0 now
where the time goes in v1:
time: 199 us
  Pallas kernels  163 us (82%)
  matrix products  9.7 us (5%)
  other arithmetic  8.36 us (4%)
  local copies, waits for them, and re-layouts  7.14 us (4%)
  starting transfers between devices  6.07 us (3%)
  waiting for transfers between devices  4.51 us (2%)
    pallas_call x1, Pallas kernels, routed_by_plane(): pl.pallas_call(functools.partial(layer_kernel, planes, stride, tps, cap),...  163 us
    ppermute x1, waiting for transfers between devices, shards(): lax.ppermute(lax.dynamic_slice_in_dim(attended, (1 - tp) * half, half, 0)...  4.5 us
    unnamed x15, local copies, waits for them, and re-layouts  4.4 us
  transfers between devices with their start and end apart: 3, of which 1 were waited for; matrix products, arithmetic and copies ran while one was open for 3% of the time, Pallas kernels for 0%

profile of v1, /device:TPU:0, one launch (start us, length us, event | category | flops | bytes accessed | tf_op | source)
XLA Modules:
  0.0 199.0 jit_solution(11781533924553028597)
XLA Ops:
  0.0 0.0 copy-start.3
  0.0 1.1 copy.26
  1.1 0.7 convert_element_type.46
  1.9 2.4 %collective-permute-start = (bf16[128,384]{0,1:T(8,128)(2,1)S(1)}, bf16[128,384]{0,1:T(8,128)(2,1)S(1)}, u32[]{:S(2)}, u32[]{:S(2)}) collective-permute-start(bf16[128,384]{0,1:T(8,128)(2,1)S(1)} %get-tuple-element.21), channel_id=1, source_target_pairs={{0,2},{2,4},{4,6},{6,8},{8,10},{10,12},{12,14},{14,16},{16,18},{18... | collective-permute-start | bytes 294920 | tf_op jit(solution)/shard_map/ppermute | solution.py:23
  4.3 1.3 collective-permute-start.1
  5.6 0.8 copy.19
  6.4 0.1 eq.57
  6.5 0.1 eq.53
  6.7 1.3 copy.17
  8.0 0.7 max.22
  8.7 1.2 reduce-window.6
  9.9 0.2 slice_reduce_fusion
  10.2 0.1 fusion.15
  10.3 0.1 sub.66
  10.4 0.1 copy.22
  10.5 0.0 collective-permute-done
  10.5 0.0 collective-permute-done.1
  10.5 0.1 pad_maximum_fusion
  10.7 0.0 copy-done.3
  10.7 0.9 fusion.8
  11.6 2.1 %fusion = (f32[2,4,512]{2,1,0:T(4,128)S(1)}, f32[2,768,512,4]{2,1,3,0:T(8,128)S(1)}) fusion(pred[512,768]{0,1:T(8,128)(4,1)S(1)} %fusion.8, bf16[512,2,4,64]{0,3,2,1:T(8,128)(2,1)S(1)} %bitcast.60, bf16[768,2,128]{0,2,1:T(8,128)(2,1)S(1)} %bitcast.61), kind=kOutput, calls=%fused_computation.3 | convolution fusion | flops 412086272 | bytes 13713408 | tf_op jit(solution)/shard_map/while/body/eval_jaxpr/qhgd,khd->hgqk/dot_general | solution.py:462
  13.7 0.1 broadcast_maximum_fusion
  13.7 3.1 %fusion.1 = f32[2,4,512]{2,1,0:T(4,128)S(1)} fusion(f32[2,768,512,4]{2,1,3,0:T(8,128)S(1)} %get-tuple-element.32, f32[2,4,512]{2,1,0:T(4,128)S(1)} %broadcast_maximum_fusion, pred[512,768]{0,1:T(8,128)(4,1)S(1)} %fusion.8), kind=kLoop, calls=%fused_computation.4 | loop fusion | flops 15724544 | bytes 13008896 | tf_op jit(solution)/shard_map/while/body/eval_jaxpr/reduce_sum | solution.py:476
  16.8 0.1 exponential_add_fusion
  16.9 0.0 copy-start.2
  16.9 0.0 copy-start.4
  16.9 0.0 copy-start.5
  16.9 4.0 %fusion.9 = bf16[2,64,4,512]{3,1,2,0:T(8,128)(2,1)S(1)} fusion(f32[2,768,512,4]{2,1,3,0:T(8,128)S(1)} %get-tuple-element.32, f32[2,4,512]{2,1,0:T(4,128)S(1)} %exponential_add_fusion, f32[2,4,512]{2,1,0:T(4,128)S(1)} %broadcast_maximum_fusion, pred[512,768]{0,1:T(8,128)(4,1)S(1)} %fusion.8, bf16[768,2,128]{0,2,1:T(8,128)(2,1)S(1)} %bitcast.62), kind=kOutput, calls=%fused_computation.16 | convolution fusion | flops 421789696 | bytes 13729792 | tf_op jit(solution)/shard_map/while/body/eval_jaxpr/hgqk,khd->qhgd/dot_general | solution.py:478
  21.0 2.4 %collective-permute-start.2 = (bf16[256,512]{0,1:T(8,128)(2,1)S(1)}, bf16[256,512]{0,1:T(8,128)(2,1)S(1)}, u32[]{:S(2)}, u32[]{:S(2)}) collective-permute-start(bf16[256,512]{0,1:T(8,128)(2,1)S(1)} %constant_dynamic-slice_fusion), channel_id=1, source_target_pairs={{0,1},{1,0},{2,3},{3,2},{4,5},{5,4},{6,7},{7,6},{8,9},{9,8},{10,11... | collective-permute-start | bytes 786440 | tf_op jit(solution)/shard_map/ppermute | solution.py:490
  23.3 0.0 copy-done.2
  23.4 0.1 pad.2.clone
  23.4 0.0 copy-done.4
  23.4 0.7 maximum_maximum_fusion.tab_ref
  24.1 4.5 %collective-permute-done.2 = bf16[256,512]{0,1:T(8,128)(2,1)S(1)} collective-permute-done((bf16[256,512]{0,1:T(8,128)(2,1)S(1)}, bf16[256,512]{0,1:T(8,128)(2,1)S(1)}, u32[]{:S(2)}, u32[]{:S(2)}) %collective-permute-start.2) | collective-permute-done | bytes 262176 | tf_op jit(solution)/shard_map/ppermute | solution.py:490
  28.6 0.1 broadcast_select_fusion.1
  28.7 0.0 copy-done.5
  28.8 0.0 copy-start.1
  28.8 3.6 %fusion.4 = (f32[256]{0:T(256)S(1)}, bf16[256,2048]{1,0:T(8,128)(2,1)S(1)}) fusion(bf16[1024,2048]{1,0:T(8,128)(2,1)} %param.16, bf16[256,512]{0,1:T(8,128)(2,1)S(1)} %get-tuple-element.20, bf16[256,512]{0,1:T(8,128)(2,1)S(1)} %get-tuple-element.19, bf16[256,2048]{1,0:T(8,128)(2,1)S(1)} %copy-done.5), kind=kOutput, calls=%fused_computation.10 | convolution fusion | flops 1077935872 | bytes 6816768 | tf_op jit(solution)/shard_map/dot_general | solution.py:498
  32.4 0.0 copy-start
  32.4 0.0 copy-done.1
  32.4 1.3 fusion.6.x_ref
  33.7 0.0 copy-done
  33.7 163.0 %routed.1 = bf16[256,2048]{1,0:T(8,128)(2,1)} custom-call(bf16[256,2048]{1,0:T(8,128)(2,1)} %fusion.6.x_ref, f32[8,256]{1,0:T(8,128)} %maximum_maximum_fusion.tab_ref, bf16[256,2048]{1,0:T(8,128)(2,1)} %copy-done, bf16[2048,1024]{1,0:T(8,128)(2,1)} %bitcast.54, bf16[2048,1024]{1,0:T(8,128)(2,1)} %bitcast.55, bf16[1024,2048]{1,0:T(8,128)(2,1)} %bitcast.56), custom_call_target="tpu_custom_call" | custom-call | tf_op jit(solution)/shard_map/routed/pallas_call | solution.py:392
  196.7 2.3 %copy.30 = bf16[256,2048]{1,0:T(8,128)(2,1)} copy(bf16[256,2048]{1,0:T(8,128)(2,1)} %routed.1) | data formatting | bytes 2097152
  (15 shorter events, 0.2 us)
Async XLA Ops:
  0.0 10.7 %copy-start.3 = (s32[512]{0:T(512)S(1)}, s32[512]{0:T(512)}, u32[]{:S(2)}) copy-start(s32[512]{0:T(512)} %param.14) | copy-start | bytes 6148
  1.9 8.7 %collective-permute-start = (bf16[128,384]{0,1:T(8,128)(2,1)S(1)}, bf16[128,384]{0,1:T(8,128)(2,1)S(1)}, u32[]{:S(2)}, u32[]{:S(2)}) collective-permute-start(bf16[128,384]{0,1:T(8,128)(2,1)S(1)} %get-tuple-element.21), channel_id=1, source_target_pairs={{0,2},{2,4},{4,6},{6,8},{8,10},{10,12},{12,14},{14,16},{16,18},{18... | collective-permute-start | bytes 294920 | tf_op jit(solution)/shard_map/ppermute | solution.py:23
  4.3 6.3 %collective-permute-start.1 = (bf16[128,384]{0,1:T(8,128)(2,1)S(1)}, bf16[128,384]{0,1:T(8,128)(2,1)S(1)}, u32[]{:S(2)}, u32[]{:S(2)}) collective-permute-start(bf16[128,384]{0,1:T(8,128)(2,1)S(1)} %get-tuple-element.22), channel_id=1, source_target_pairs={{2,0},{4,2},{6,4},{8,6},{10,8},{12,10},{14,12},{16,14},{18,16},{20... | collective-permute-start | bytes 294920 | tf_op jit(solution)/shard_map/ppermute | solution.py:25
  16.9 6.4 %copy-start.2 = (s32[256,2]{0,1:T(2,128)S(1)}, s32[256,2]{0,1:T(2,128)}, u32[]{:S(2)}) copy-start(s32[256,2]{0,1:T(2,128)} %param.22) | copy-start | bytes 6148
  16.9 6.5 %copy-start.4 = (f32[256,2]{0,1:T(2,128)S(1)}, f32[256,2]{0,1:T(2,128)}, u32[]{:S(2)}) copy-start(f32[256,2]{0,1:T(2,128)} %param.23) | copy-start | bytes 6148
  16.9 11.8 %copy-start.5 = (bf16[256,2048]{1,0:T(8,128)(2,1)S(1)}, bf16[256,2048]{1,0:T(8,128)(2,1)}, u32[]{:S(2)}) copy-start(bf16[256,2048]{1,0:T(8,128)(2,1)} %param.17) | copy-start | bytes 3145732
  21.0 7.6 %collective-permute-start.2 = (bf16[256,512]{0,1:T(8,128)(2,1)S(1)}, bf16[256,512]{0,1:T(8,128)(2,1)S(1)}, u32[]{:S(2)}, u32[]{:S(2)}) collective-permute-start(bf16[256,512]{0,1:T(8,128)(2,1)S(1)} %constant_dynamic-slice_fusion), channel_id=1, source_target_pairs={{0,1},{1,0},{2,3},{3,2},{4,5},{5,4},{6,7},{7,6},{8,9},{9,8},{10,11... | collective-permute-start | bytes 786440 | tf_op jit(solution)/shard_map/ppermute | solution.py:490
  28.8 3.7 %copy-start.1 = (f32[2048]{0:T(1024)S(1)}, f32[2048]{0:T(1024)}, u32[]{:S(2)}) copy-start(f32[2048]{0:T(1024)} %param.18) | copy-start | bytes 24580
  32.4 1.3 copy-start

commit v2 on v1

--- a/solution.py
+++ b/solution.py
@@ -10,8 +10,11 @@
 HD = 64
 WIN = 128
 PLANES = 4
-CUTS = 4
+CUTS = 8
 TILE = 256
+LAND_LAG = 2
+HELD_LAG = 2
+FAR_LAG = 2
 MESH = pl.DeviceIdType.MESH
 
 
@@ -72,7 +75,7 @@
     planes, stride, tps, cap,
     x_ref, tab_ref, mid_ref, gate_ref, up_ref, down_ref, out_ref,
     toks, stage, land, results, held, part, from_low, from_high,
-    gate_w, up_w, down_w, hidden, mixer, total, tabs,
+    gate_w, up_w, down_w, gate_sum, up_sum, hidden, mixer, total, tabs,
     zsend, zrecv, psend, precv, rsend, rrecv, csend, lowrecv, highrecv, tsend, trecv, wsem,
 ):
     z, r, tp, p = place(stride, tps)
@@ -81,7 +84,13 @@
     cols = width // CUTS
     slots = peers * cap
     near = planes - 1
+    packed = planes * CUTS
     greet(z, r, tp, p, planes, stride, tps)
+
+    def block(b):
+        inward = jnp.where(z < planes // 2, z + b, z - b)
+        outward = jnp.where(z < planes // 2, z - 1, z + 1)
+        return jnp.where((inward >= 0) & (inward < planes), inward, outward)
 
     def span(h):
         return pl.ds(pl.multiple_of(h * cols, cols), cols)
@@ -172,77 +181,102 @@
         )
     ]
 
-    def pack(block, zs, h):
+    def pack(zs, h):
         first, second = slot_hits(tabs[zs], z, slots, rows)
         pick = jnp.where(first | second, 1.0, 0.0).astype(jnp.bfloat16)
-        picked = jnp.dot(pick, block, preferred_element_type=jnp.float32)
+        picked = jnp.dot(pick, toks[zs, :, span(h)], preferred_element_type=jnp.float32)
         stage[zs, :, span(h)] = picked.astype(jnp.bfloat16)
         for k in range(1, peers):
             give(zs, h, lax.rem(p + k, peers), p).start()
         land[zs, seat(p), span(h)] = stage[zs, seat(p), span(h)]
 
-    def experts(zs):
-        tab = tabs[zs]
-        first, second = slot_hits(tab, z, slots, rows)
-        mix = jnp.where(first, tab[2:3, :], 0.0) + jnp.where(second, tab[3:4, :], 0.0)
-        mixer[zs] = mix.T.astype(jnp.bfloat16)
-
-        @pl.loop(0, CUTS)
-        def _(h):
-            for k in range(1, peers):
-                other = lax.rem(p + k, peers)
-                give(zs, h, other, other).wait_recv()
+    def expand(zs, h):
+        @pl.when(h == 0)
+        def _():
+            tab = tabs[zs]
+            first, second = slot_hits(tab, z, slots, rows)
+            mix = jnp.where(first, tab[2:3, :], 0.0) + jnp.where(second, tab[3:4, :], 0.0)
+            mixer[zs] = mix.T.astype(jnp.bfloat16)
+            gate_sum[...] = jnp.zeros_like(gate_sum)
+            up_sum[...] = jnp.zeros_like(up_sum)
+
+        for k in range(1, peers):
+            other = lax.rem(p + k, peers)
+            give(zs, h, other, other).wait_recv()
 
         @pl.loop(0, gate_w.shape[1] // TILE)
         def _(c):
             at = pl.ds(pl.multiple_of(c * TILE, TILE), TILE)
-            gate = jnp.dot(land[zs], gate_w[:, at], preferred_element_type=jnp.float32)
-            upper = jnp.dot(land[zs], up_w[:, at], preferred_element_type=jnp.float32)
-            hidden[:, at] = (gate / (1.0 + jnp.exp(-gate)) * upper).astype(jnp.bfloat16)
-
-        @pl.loop(0, CUTS)
-        def _(h):
-            @pl.loop(0, cols // TILE)
+            here = land[zs, :, span(h)]
+            gate_sum[:, at] += jnp.dot(
+                here, gate_w[span(h), at], preferred_element_type=jnp.float32
+            )
+            up_sum[:, at] += jnp.dot(here, up_w[span(h), at], preferred_element_type=jnp.float32)
+
+        @pl.when(h == CUTS - 1)
+        def _():
+            @pl.loop(0, gate_w.shape[1] // TILE)
             def _(c):
-                at = pl.ds(pl.multiple_of(h * cols + c * TILE, TILE), TILE)
-                results[zs, :, at] = jnp.dot(
-                    hidden[...], down_w[:, at], preferred_element_type=jnp.float32
-                ).astype(jnp.bfloat16)
-
-            for k in range(1, peers):
-                back(zs, h, lax.rem(p + k, peers), p).start()
-            held[zs, seat(p), span(h)] = results[zs, seat(p), span(h)]
+                at = pl.ds(pl.multiple_of(c * TILE, TILE), TILE)
+                gate = gate_sum[:, at]
+                hidden[:, at] = (gate / (1.0 + jnp.exp(-gate)) * up_sum[:, at]).astype(
+                    jnp.bfloat16
+                )
+
+    def contract(zs, h):
+        results[zs, :, span(h)] = jnp.dot(
+            hidden[...], down_w[:, span(h)], preferred_element_type=jnp.float32
+        ).astype(jnp.bfloat16)
+
+    def send_back(zs, h):
+        for k in range(1, peers):
+            back(zs, h, lax.rem(p + k, peers), p).start()
+        held[zs, seat(p), span(h)] = results[zs, seat(p), span(h)]
 
     def mixed(zs, h):
         for k in range(1, peers):
             back(zs, h, p, lax.rem(p + k, peers)).wait_recv()
         return jnp.dot(mixer[zs], held[zs, :, span(h)], preferred_element_type=jnp.float32)
 
-    def homeward(stage_of, h):
+    def homeward(f):
         @pl.loop(0, 2)
         def _(k):
             down = (k == 0) == (z >= planes // 2)
-            zs = jnp.where(down, near - stage_of, stage_of)
-
-            @pl.when(down & (zs < z))
+            g = f - FAR_LAG * k
+            round_of = lax.div(g, CUTS) + 1
+            h = lax.rem(g, CUTS)
+            zs = jnp.where(down, near - round_of, round_of)
+            due = (g >= 0) & (g < near * CUTS)
+
+            @pl.when(due & down & (zs < z))
             def _():
-                part[zs, :, span(h)] = mixed(zs, h).astype(jnp.bfloat16)
+                mine = mixed(zs, h)
+
+                @pl.when(z == near)
+                def _():
+                    part[zs, :, span(h)] = mine.astype(jnp.bfloat16)
 
                 @pl.when(z < near)
                 def _():
                     sink(zs, h).wait_recv()
-                    part[zs, :, span(h)] += from_high[zs, :, span(h)]
+                    above = from_high[zs, :, span(h)].astype(jnp.float32)
+                    part[zs, :, span(h)] = (mine + above).astype(jnp.bfloat16)
 
                 sink(zs, h).start()
 
-            @pl.when(jnp.logical_not(down) & (zs > z))
+            @pl.when(due & jnp.logical_not(down) & (zs > z))
             def _():
-                part[zs, :, span(h)] = mixed(zs, h).astype(jnp.bfloat16)
+                mine = mixed(zs, h)
+
+                @pl.when(z == 0)
+                def _():
+                    part[zs, :, span(h)] = mine.astype(jnp.bfloat16)
 
                 @pl.when(z > 0)
                 def _():
                     climb(zs, h).wait_recv()
-                    part[zs, :, span(h)] += from_low[zs, :, span(h)]
+                    below = from_low[zs, :, span(h)].astype(jnp.float32)
+                    part[zs, :, span(h)] = (mine + below).astype(jnp.bfloat16)
 
                 climb(zs, h).start()
 
@@ -268,65 +302,68 @@
         load.start()
     tabs[z] = tab_ref[...]
 
+    toks[z] = x_ref[...]
+
     @pl.loop(0, CUTS)
     def _(h):
-        pack(x_ref[:, span(h)], z, h)
+        pack(z, h)
 
     for load in loads:
         load.wait()
 
-    @pl.loop(CUTS, (planes + 1) * CUTS)
+    def turn(k):
+        nth = lax.div(k, CUTS)
+        return jnp.where(nth < near, block(nth + 1), z), lax.rem(k, CUTS)
+
+    @pl.loop(0, packed + LAND_LAG + CUTS - 1)
     def _(e):
-        dist = lax.div(e, CUTS)
+        dist = lax.div(e, CUTS) + 1
         h = lax.rem(e, CUTS)
 
-        @pl.loop(0, 2)
-        def _(side):
-            zs = z - dist + 2 * dist * side
-            onward = z + 1 - 2 * side
-
-            @pl.when((zs >= 0) & (zs < planes))
-            def _():
-                @pl.when(h == 0)
+        @pl.when(dist <= near)
+        def _():
+            @pl.loop(0, 2)
+            def _(side):
+                zs = z - dist + 2 * dist * side
+                onward = z + 1 - 2 * side
+
+                @pl.when((zs >= 0) & (zs < planes))
                 def _():
-                    tab_hop(zs, side, tabs.at[zs]).wait_recv()
+                    @pl.when(h == 0)
+                    def _():
+                        tab_hop(zs, side, tabs.at[zs]).wait_recv()
+
+                        @pl.when((onward >= 0) & (onward < planes))
+                        def _():
+                            tab_hop(zs, side, tabs.at[zs]).start()
+
+                    hop(zs, h, side).wait_recv()
 
                     @pl.when((onward >= 0) & (onward < planes))
                     def _():
-                        tab_hop(zs, side, tabs.at[zs]).start()
-
-                hop(zs, h, side).wait_recv()
-
-                @pl.when((onward >= 0) & (onward < planes))
-                def _():
-                    hop(zs, h, side).start()
-
-                pack(toks[zs, :, span(h)], zs, h)
-
-        @pl.when(h == 0)
-        def _():
-            @pl.loop(0, 2)
-            def _(side):
-                zs = z - (dist - 1) + 2 * (dist - 1) * side
-
-                @pl.when((zs >= 0) & (zs < planes) & ((dist > 1) | (side == 0)))
-                def _():
-                    experts(zs)
-
-        @pl.when((dist > 1) & (h > 0))
-        def _():
-            homeward(dist - 1, h - 1)
-
-        @pl.when((dist > 1) & (h == CUTS - 1))
-        def _():
-            homeward(dist - 1, h)
-
-        @pl.when(dist == planes - 1)
-        def _():
-            total[:, span(h)] = mid_ref[:, span(h)].astype(jnp.float32) + mixed(z, h)
+                        hop(zs, h, side).start()
+
+            pack(block(dist), h)
+
+        g = e - LAND_LAG
+
+        @pl.when((g >= 0) & (g < packed))
+        def _():
+            expand(*turn(g))
+
+        c = g - CUTS + 1
+
+        @pl.when(c >= 0)
+        def _():
+            contract(*turn(c))
+            send_back(*turn(c))
+
+        homeward(c - HELD_LAG)
 
     @pl.loop(0, CUTS)
     def _(h):
+        total[:, span(h)] = mid_ref[:, span(h)].astype(jnp.float32) + mixed(z, h)
+
         @pl.when(z > 0)
         def _():
             climb(z, h).wait_recv()
@@ -399,6 +436,8 @@
             pltpu.VMEM((width, hidden), jnp.bfloat16),
             pltpu.VMEM((width, hidden), jnp.bfloat16),
             pltpu.VMEM((hidden, width), jnp.bfloat16),
+            pltpu.VMEM((slots, hidden), jnp.float32),
+            pltpu.VMEM((slots, hidden), jnp.float32),
             pltpu.VMEM((slots, hidden), jnp.bfloat16),
             pltpu.VMEM((planes, rows, slots), jnp.bfloat16),
             pltpu.VMEM((rows, width), jnp.float32),

time: 199 us -> 177 us (0.89)
  the two profiles are of different devices: /device:TPU:0 before, /device:TPU:9 now
where the time goes in v2:
time: 177 us; the launch traced here: 176 us
  Pallas kernels  140 us (79%)
  matrix products  9.69 us (5%)
  other arithmetic  8.36 us (5%)
  local copies, waits for them, and re-layouts  7.14 us (4%)
  starting transfers between devices  6.91 us (4%)
  waiting for transfers between devices  4.4 us (2%)
    pallas_call x1, Pallas kernels, routed_by_plane(): pl.pallas_call(functools.partial(layer_kernel, planes, stride, tps, cap),...  140 us
    unnamed x15, local copies, waits for them, and re-layouts  4.4 us
    ppermute x1, waiting for transfers between devices, shards(): lax.ppermute(lax.dynamic_slice_in_dim(attended, (1 - tp) * half, half, 0)...  4.38 us
    dot_general x1, matrix products, one_span(): jnp.einsum('hgqk,khd->qhgd', weights, kv_ext[..., head_dim:], preferred_e...  3.98 us
    ppermute x1, starting transfers between devices, with_halo(): lax.ppermute(cells[-width:], axis, [(i, (i + 1) % count) for i in range(e...  3.71 us
    dot_general x1, matrix products, shards(): jnp.dot(gathered, out_weight, preferred_element_type=jnp.float32)  3.62 us
  transfers between devices with their start and end apart: 3, of which 1 were waited for; matrix products, arithmetic and copies ran while one was open for 3% of the time, Pallas kernels for 0%

profile of v2, /device:TPU:9, one launch (start us, length us, event | category | flops | bytes accessed | tf_op | source)
XLA Modules:
  0.0 176.4 jit_solution(17130710262518922282)
XLA Ops:
  0.0 0.0 copy-start.3
  0.0 1.1 copy.26
  1.1 0.7 convert_element_type.46
  1.9 3.7 %collective-permute-start = (bf16[128,384]{0,1:T(8,128)(2,1)S(1)}, bf16[128,384]{0,1:T(8,128)(2,1)S(1)}, u32[]{:S(2)}, u32[]{:S(2)}) collective-permute-start(bf16[128,384]{0,1:T(8,128)(2,1)S(1)} %get-tuple-element.21), channel_id=1, source_target_pairs={{0,2},{2,4},{4,6},{6,8},{8,10},{10,12},{12,14},{14,16},{16,18},{18... | collective-permute-start | bytes 294920 | tf_op jit(solution)/shard_map/ppermute | solution.py:26
  5.6 1.9 %collective-permute-start.1 = (bf16[128,384]{0,1:T(8,128)(2,1)S(1)}, bf16[128,384]{0,1:T(8,128)(2,1)S(1)}, u32[]{:S(2)}, u32[]{:S(2)}) collective-permute-start(bf16[128,384]{0,1:T(8,128)(2,1)S(1)} %get-tuple-element.22), channel_id=1, source_target_pairs={{2,0},{4,2},{6,4},{8,6},{10,8},{12,10},{14,12},{16,14},{18,16},{20... | collective-permute-start | bytes 294920 | tf_op jit(solution)/shard_map/ppermute | solution.py:28
  7.5 0.8 copy.19
  8.3 0.1 eq.57
  8.5 0.1 eq.53
  8.6 1.3 copy.17
  9.9 0.7 max.22
  10.7 1.2 reduce-window.6
  11.8 0.2 slice_reduce_fusion
  12.1 0.1 fusion.15
  12.2 0.1 sub.66
  12.4 0.1 copy.22
  12.4 0.0 collective-permute-done
  12.5 0.0 collective-permute-done.1
  12.5 0.1 pad_maximum_fusion
  12.6 0.0 copy-done.3
  12.6 0.9 fusion.8
  13.5 2.1 %fusion = (f32[2,4,512]{2,1,0:T(4,128)S(1)}, f32[2,768,512,4]{2,1,3,0:T(8,128)S(1)}) fusion(pred[512,768]{0,1:T(8,128)(4,1)S(1)} %fusion.8, bf16[512,2,4,64]{0,3,2,1:T(8,128)(2,1)S(1)} %bitcast.60, bf16[768,2,128]{0,2,1:T(8,128)(2,1)S(1)} %bitcast.61), kind=kOutput, calls=%fused_computation.3 | convolution fusion | flops 412086272 | bytes 13713408 | tf_op jit(solution)/shard_map/while/body/eval_jaxpr/qhgd,khd->hgqk/dot_general | solution.py:501
  15.6 0.1 broadcast_maximum_fusion
  15.7 3.1 %fusion.1 = f32[2,4,512]{2,1,0:T(4,128)S(1)} fusion(f32[2,768,512,4]{2,1,3,0:T(8,128)S(1)} %get-tuple-element.32, f32[2,4,512]{2,1,0:T(4,128)S(1)} %broadcast_maximum_fusion, pred[512,768]{0,1:T(8,128)(4,1)S(1)} %fusion.8), kind=kLoop, calls=%fused_computation.4 | loop fusion | flops 15724544 | bytes 13008896 | tf_op jit(solution)/shard_map/while/body/eval_jaxpr/reduce_sum | solution.py:515
  18.8 0.1 exponential_add_fusion
  18.8 0.0 copy-start.2
  18.9 0.0 copy-start.4
  18.9 0.0 copy-start.5
  18.9 4.0 %fusion.9 = bf16[2,64,4,512]{3,1,2,0:T(8,128)(2,1)S(1)} fusion(f32[2,768,512,4]{2,1,3,0:T(8,128)S(1)} %get-tuple-element.32, f32[2,4,512]{2,1,0:T(4,128)S(1)} %exponential_add_fusion, f32[2,4,512]{2,1,0:T(4,128)S(1)} %broadcast_maximum_fusion, pred[512,768]{0,1:T(8,128)(4,1)S(1)} %fusion.8, bf16[768,2,128]{0,2,1:T(8,128)(2,1)S(1)} %bitcast.62), kind=kOutput, calls=%fused_computation.16 | convolution fusion | flops 421789696 | bytes 13729792 | tf_op jit(solution)/shard_map/while/body/eval_jaxpr/hgqk,khd->qhgd/dot_general | solution.py:517
  22.9 1.3 collective-permute-start.2
  24.2 0.0 copy-done.2
  24.2 0.1 pad.2.clone
  24.3 0.0 copy-done.4
  24.3 0.7 maximum_maximum_fusion.tab_ref
  24.9 4.4 %collective-permute-done.2 = bf16[256,512]{0,1:T(8,128)(2,1)S(1)} collective-permute-done((bf16[256,512]{0,1:T(8,128)(2,1)S(1)}, bf16[256,512]{0,1:T(8,128)(2,1)S(1)}, u32[]{:S(2)}, u32[]{:S(2)}) %collective-permute-start.2) | collective-permute-done | bytes 262176 | tf_op jit(solution)/shard_map/ppermute | solution.py:529
  29.3 0.1 broadcast_select_fusion.1
  29.5 0.0 copy-done.5
  29.5 0.0 copy-start.1
  29.5 3.6 %fusion.4 = (f32[256]{0:T(256)S(1)}, bf16[256,2048]{1,0:T(8,128)(2,1)S(1)}) fusion(bf16[1024,2048]{1,0:T(8,128)(2,1)} %param.16, bf16[256,512]{0,1:T(8,128)(2,1)S(1)} %get-tuple-element.20, bf16[256,512]{0,1:T(8,128)(2,1)S(1)} %get-tuple-element.19, bf16[256,2048]{1,0:T(8,128)(2,1)S(1)} %copy-done.5), kind=kOutput, calls=%fused_computation.10 | convolution fusion | flops 1077935872 | bytes 6816768 | tf_op jit(solution)/shard_map/dot_general | solution.py:537
  33.1 0.0 copy-start
  33.1 0.0 copy-done.1
  33.1 1.3 fusion.6.x_ref
  34.4 0.0 copy-done
  34.4 139.7 %routed.1 = bf16[256,2048]{1,0:T(8,128)(2,1)} custom-call(bf16[256,2048]{1,0:T(8,128)(2,1)} %fusion.6.x_ref, f32[8,256]{1,0:T(8,128)} %maximum_maximum_fusion.tab_ref, bf16[256,2048]{1,0:T(8,128)(2,1)} %copy-done, bf16[2048,1024]{1,0:T(8,128)(2,1)} %bitcast.54, bf16[2048,1024]{1,0:T(8,128)(2,1)} %bitcast.55, bf16[1024,2048]{1,0:T(8,128)(2,1)} %bitcast.56), custom_call_target="tpu_custom_call" | custom-call | tf_op jit(solution)/shard_map/routed/pallas_call | solution.py:429
  174.1 2.3 %copy.30 = bf16[256,2048]{1,0:T(8,128)(2,1)} copy(bf16[256,2048]{1,0:T(8,128)(2,1)} %routed.1) | data formatting | bytes 2097152
  (15 shorter events, 0.2 us)
Async XLA Ops:
  0.0 12.6 %copy-start.3 = (s32[512]{0:T(512)S(1)}, s32[512]{0:T(512)}, u32[]{:S(2)}) copy-start(s32[512]{0:T(512)} %param.14) | copy-start | bytes 6148
  1.9 10.6 %collective-permute-start = (bf16[128,384]{0,1:T(8,128)(2,1)S(1)}, bf16[128,384]{0,1:T(8,128)(2,1)S(1)}, u32[]{:S(2)}, u32[]{:S(2)}) collective-permute-start(bf16[128,384]{0,1:T(8,128)(2,1)S(1)} %get-tuple-element.21), channel_id=1, source_target_pairs={{0,2},{2,4},{4,6},{6,8},{8,10},{10,12},{12,14},{14,16},{16,18},{18... | collective-permute-start | bytes 294920 | tf_op jit(solution)/shard_map/ppermute | solution.py:26
  5.6 6.9 %collective-permute-start.1 = (bf16[128,384]{0,1:T(8,128)(2,1)S(1)}, bf16[128,384]{0,1:T(8,128)(2,1)S(1)}, u32[]{:S(2)}, u32[]{:S(2)}) collective-permute-start(bf16[128,384]{0,1:T(8,128)(2,1)S(1)} %get-tuple-element.22), channel_id=1, source_target_pairs={{2,0},{4,2},{6,4},{8,6},{10,8},{12,10},{14,12},{16,14},{18,16},{20... | collective-permute-start | bytes 294920 | tf_op jit(solution)/shard_map/ppermute | solution.py:28
  18.8 5.3 %copy-start.2 = (s32[256,2]{0,1:T(2,128)S(1)}, s32[256,2]{0,1:T(2,128)}, u32[]{:S(2)}) copy-start(s32[256,2]{0,1:T(2,128)} %param.22) | copy-start | bytes 6148
  18.9 5.4 %copy-start.4 = (f32[256,2]{0,1:T(2,128)S(1)}, f32[256,2]{0,1:T(2,128)}, u32[]{:S(2)}) copy-start(f32[256,2]{0,1:T(2,128)} %param.23) | copy-start | bytes 6148
  18.9 10.6 %copy-start.5 = (bf16[256,2048]{1,0:T(8,128)(2,1)S(1)}, bf16[256,2048]{1,0:T(8,128)(2,1)}, u32[]{:S(2)}) copy-start(bf16[256,2048]{1,0:T(8,128)(2,1)} %param.17) | copy-start | bytes 3145732
  22.9 6.4 %collective-permute-start.2 = (bf16[256,512]{0,1:T(8,128)(2,1)S(1)}, bf16[256,512]{0,1:T(8,128)(2,1)S(1)}, u32[]{:S(2)}, u32[]{:S(2)}) collective-permute-start(bf16[256,512]{0,1:T(8,128)(2,1)S(1)} %constant_dynamic-slice_fusion), channel_id=1, source_target_pairs={{0,1},{1,0},{2,3},{3,2},{4,5},{5,4},{6,7},{7,6},{8,9},{9,8},{10,11... | collective-permute-start | bytes 786440 | tf_op jit(solution)/shard_map/ppermute | solution.py:529
  29.5 3.7 %copy-start.1 = (f32[2048]{0:T(1024)S(1)}, f32[2048]{0:T(1024)}, u32[]{:S(2)}) copy-start(f32[2048]{0:T(1024)} %param.18) | copy-start | bytes 24580
  33.1 1.3 copy-start

commit v3 on v2

--- a/solution.py
+++ b/solution.py
@@ -8,6 +8,7 @@
 from jax.sharding import PartitionSpec as P
 
 HD = 64
+LANES = 128
 WIN = 128
 PLANES = 4
 CUTS = 8
@@ -61,8 +62,25 @@
             barrier, inc=1, device_id=((z + 1) * stride + r, tp), device_id_type=MESH
         )
 
-    beside = (z > 0).astype(jnp.int32) + (z < planes - 1).astype(jnp.int32)
-    pl.semaphore_wait(barrier, peers - 1 + beside)
+    first = (z > 0) & (r == 0)
+    last = (z < planes - 1) & (r == stride - 1)
+
+    @pl.when(first)
+    def _():
+        pl.semaphore_signal(
+            barrier, inc=1, device_id=(z * stride - 1, tp), device_id_type=MESH
+        )
+
+    @pl.when(last)
+    def _():
+        pl.semaphore_signal(
+            barrier, inc=1, device_id=((z + 1) * stride, tp), device_id_type=MESH
+        )
+
+    count = peers - 1
+    for there in (z > 0, z < planes - 1, first, last):
+        count = count + there.astype(jnp.int32)
+    pl.semaphore_wait(barrier, count)
 
 
 def slot_hits(tab, z, slots, rows):
@@ -73,19 +91,200 @@
 
 def layer_kernel(
     planes, stride, tps, cap,
-    x_ref, tab_ref, mid_ref, gate_ref, up_ref, down_ref, out_ref,
+    q_ref, slab_ref, sink_ref, gain_ref, routes_ref, share_ref,
+    out_w_ref, hidden_in_ref, gate_ref, up_ref, down_ref, out_ref,
+    reach, outbox, gathered, out_w, resid, bias, squares,
     toks, stage, land, results, held, part, from_low, from_high,
     gate_w, up_w, down_w, gate_sum, up_sum, hidden, mixer, total, tabs,
     zsend, zrecv, psend, precv, rsend, rrecv, csend, lowrecv, highrecv, tsend, trecv, wsem,
+    hsend, hrecv, xsend, xrecv, ssem,
 ):
     z, r, tp, p = place(stride, tps)
     peers = stride * tps
-    rows, width = x_ref.shape
+    rows, width = out_ref.shape
     cols = width // CUTS
     slots = peers * cap
     near = planes - 1
     packed = planes * CUTS
+    sp = z * stride + r
+    ends = planes * stride - 1
+    tok_here, heads_wide = q_ref.shape
+    kv_wide = slab_ref.shape[1] - LANES
+    starts = [
+        pltpu.make_async_copy(source, target, ssem.at[k])
+        for k, (source, target) in enumerate([(out_w_ref, out_w), (hidden_in_ref, resid)])
+    ]
+    loads = [
+        pltpu.make_async_copy(source, target, wsem.at[k])
+        for k, (source, target) in enumerate(
+            [(gate_ref, gate_w), (up_ref, up_w), (down_ref, down_w)]
+        )
+    ]
+    for load in starts:
+        load.start()
     greet(z, r, tp, p, planes, stride, tps)
+
+    def halo(side):
+        there = 0 if side else tok_here + WIN
+        return pltpu.make_async_remote_copy(
+            src_ref=slab_ref.at[pl.ds((tok_here - WIN) * side, WIN), :],
+            dst_ref=reach.at[pl.ds(there, WIN), :],
+            send_sem=hsend.at[side],
+            recv_sem=hrecv.at[side],
+            device_id=(sp - 1 + 2 * side, tp),
+            device_id_type=MESH,
+        )
+
+    def swap(k, at):
+        return pltpu.make_async_remote_copy(
+            src_ref=outbox.at[k],
+            dst_ref=gathered.at[
+                pl.ds(pl.multiple_of(at * WIN, WIN), WIN),
+                pl.ds(pl.multiple_of(tp * heads_wide, LANES), heads_wide),
+            ],
+            send_sem=xsend.at[k],
+            recv_sem=xrecv.at[k],
+            device_id=(sp, 1 - tp),
+            device_id_type=MESH,
+        )
+
+    for side in range(2):
+
+        @pl.when((sp < ends) if side else (sp > 0))
+        def _():
+            halo(side).start()
+
+    for load in loads:
+        load.start()
+
+    @pl.when(sp == 0)
+    def _():
+        reach[0:WIN, :] = jnp.zeros((WIN, reach.shape[1]), reach.dtype)
+
+    @pl.when(sp == ends)
+    def _():
+        reach[tok_here + WIN :, :] = jnp.zeros((WIN, reach.shape[1]), reach.dtype)
+
+    reach[WIN : tok_here + WIN, :] = slab_ref[...]
+    picks = routes_ref[...]
+    expert = lax.broadcasted_iota(jnp.int32, (planes * peers, rows), 0)
+    early = lax.broadcasted_iota(jnp.int32, (rows, rows), 0) < lax.broadcasted_iota(
+        jnp.int32, (rows, rows), 1
+    )
+    chosen = [jnp.where(expert == picks[k : k + 1, :], 1.0, 0.0) for k in range(2)]
+    ahead = jnp.dot(
+        (chosen[0] + chosen[1]).astype(jnp.bfloat16),
+        jnp.where(early, 1.0, 0.0).astype(jnp.bfloat16),
+        preferred_element_type=jnp.float32,
+    )
+    for k in range(2):
+        place_in = jnp.sum(chosen[k] * ahead, axis=0, keepdims=True)
+        tabs[z, k : k + 1, :] = picks[k : k + 1, :].astype(jnp.float32) * cap + place_in
+        tabs[z, k + 2 : k + 3, :] = share_ref[k : k + 1, :]
+    tabs[z, 4:8, :] = jnp.zeros((4, rows), jnp.float32)
+
+    halves = rows // WIN
+    span_keys = 3 * WIN
+    nt = (((1,), (1,)), ((), ()))
+
+    def attend(b, out_at):
+        near_rows = pl.ds(pl.multiple_of(b * WIN, WIN), WIN)
+        window = pl.ds(pl.multiple_of(b * WIN, WIN), span_keys)
+        middle = pl.ds(pl.multiple_of(b * WIN + WIN, WIN), WIN)
+        same = lax.dot_general(
+            reach[middle, kv_wide:], reach[window, kv_wide:], nt,
+            preferred_element_type=jnp.float32,
+        )
+        i = lax.broadcasted_iota(jnp.int32, (WIN, span_keys), 0)
+        j = lax.broadcasted_iota(jnp.int32, (WIN, span_keys), 1)
+        bias[...] = jnp.where((j >= i) & (j <= i + 2 * WIN) & (same > 0.5), 0.0, -1e30)
+        low_keys = lax.broadcasted_iota(jnp.int32, (span_keys, LANES), 1) < HD
+        low = lax.broadcasted_iota(jnp.int32, (WIN, LANES), 1) < HD
+        pairs = heads_wide // kv_wide
+        for g in range(kv_wide // LANES):
+            both = reach[window, g * LANES : (g + 1) * LANES].astype(jnp.float32)
+            turned = pltpu.roll(both, HD, 1)
+            keys = [
+                jnp.where(low_keys, both, 0.0).astype(jnp.bfloat16),
+                jnp.where(low_keys, 0.0, turned).astype(jnp.bfloat16),
+            ]
+            values = jnp.concatenate(
+                [
+                    jnp.where(low_keys, turned, both).astype(jnp.bfloat16),
+                    jnp.ones((span_keys, LANES), jnp.bfloat16),
+                ],
+                axis=1,
+            )
+            for pair in range(pairs):
+                at = (g * pairs + pair) * LANES
+                query = q_ref[near_rows, at : at + LANES] * jnp.bfloat16(HD**-0.5)
+                done = []
+                for odd in range(2):
+                    sink = sink_ref[(g * pairs + pair) * 2 + odd]
+                    score = lax.dot_general(
+                        query, keys[odd], nt, preferred_element_type=jnp.float32
+                    )
+                    score = score + bias[...]
+                    row_max = jnp.maximum(jnp.max(score, axis=1, keepdims=True), sink)
+                    weight = jnp.exp(score - row_max).astype(jnp.bfloat16)
+                    outcome = jnp.dot(weight, values, preferred_element_type=jnp.float32)
+                    mass = outcome[:, LANES:] + jnp.exp(sink - row_max)
+                    done.append(outcome[:, :LANES] / mass)
+                out_at(at)[...] = jnp.where(low, done[0], done[1]).astype(jnp.bfloat16)
+
+    def block_of(k):
+        return jnp.where(
+            tp == 0,
+            jnp.where(k < halves, halves + k, 2 * halves - 1 - k),
+            jnp.where(k < halves, halves - 1 - k, k),
+        )
+
+    @pl.loop(0, 2 * halves)
+    def _(k):
+        b = block_of(k)
+
+        @pl.when((b == 0) & (sp > 0))
+        def _():
+            halo(1).wait_recv()
+
+        @pl.when((b == 2 * halves - 1) & (sp < ends))
+        def _():
+            halo(0).wait_recv()
+
+        box = jnp.minimum(k, halves)
+        attend(b, lambda at: outbox.at[box, :, pl.ds(at, LANES)])
+
+        @pl.when(k < halves)
+        def _():
+            swap(k, b - halves * (1 - tp)).start()
+
+        @pl.when(k >= halves)
+        def _():
+            gathered[
+                pl.ds(pl.multiple_of((b - halves * tp) * WIN, WIN), WIN),
+                pl.ds(pl.multiple_of(tp * heads_wide, LANES), heads_wide),
+            ] = outbox[halves]
+
+    for load in starts:
+        load.wait()
+    squares[...] = jnp.zeros_like(squares)
+    for k in range(halves):
+        swap(k, 0).wait_recv()
+
+    @pl.loop(0, width // TILE)
+    def _(c):
+        at = pl.ds(pl.multiple_of(c * TILE, TILE), TILE)
+        mid = resid[:, at].astype(jnp.float32) + jnp.dot(
+            gathered[...], out_w[:, at], preferred_element_type=jnp.float32
+        )
+        mid = mid.astype(jnp.bfloat16).astype(jnp.float32)
+        total[:, at] = mid
+        square = mid * mid
+        for k in range(TILE // LANES):
+            squares[...] += square[:, k * LANES : (k + 1) * LANES]
+
+    spread = jnp.sum(squares[...], axis=1, keepdims=True) * (1.0 / width)
+    scale = lax.rsqrt(spread + 1e-06)
 
     def block(b):
         inward = jnp.where(z < planes // 2, z + b, z - b)
@@ -114,16 +313,6 @@
             device_id_type=MESH,
         )
 
-    def own_hop(h, side):
-        return pltpu.make_async_remote_copy(
-            src_ref=x_ref.at[:, span(h)],
-            dst_ref=toks.at[z, :, span(h)],
-            send_sem=zsend.at[side, z, h],
-            recv_sem=zrecv.at[z, h],
-            device_id=beside(side),
-            device_id_type=MESH,
-        )
-
     def tab_hop(zs, side, source):
         return pltpu.make_async_remote_copy(
             src_ref=source,
@@ -173,13 +362,6 @@
             device_id=beside(1),
             device_id_type=MESH,
         )
-
-    loads = [
-        pltpu.make_async_copy(source, target, wsem.at[k])
-        for k, (source, target) in enumerate(
-            [(gate_ref, gate_w), (up_ref, up_w), (down_ref, down_w)]
-        )
-    ]
 
     def pack(zs, h):
         first, second = slot_hits(tabs[zs], z, slots, rows)
@@ -282,27 +464,24 @@
 
     @pl.when(z < near)
     def _():
-        tab_hop(z, 0, tab_ref).start()
+        tab_hop(z, 0, tabs.at[z]).start()
 
     @pl.when(z > 0)
     def _():
-        tab_hop(z, 1, tab_ref).start()
-
-    for h in range(CUTS):
+        tab_hop(z, 1, tabs.at[z]).start()
+
+    @pl.loop(0, CUTS)
+    def _(h):
+        at = span(h)
+        toks[z, :, at] = (total[:, at] * scale * gain_ref[:, at]).astype(jnp.bfloat16)
 
         @pl.when(z < near)
         def _():
-            own_hop(h, 0).start()
+            hop(z, h, 0).start()
 
         @pl.when(z > 0)
         def _():
-            own_hop(h, 1).start()
-
-    for load in loads:
-        load.start()
-    tabs[z] = tab_ref[...]
-
-    toks[z] = x_ref[...]
+            hop(z, h, 1).start()
 
     @pl.loop(0, CUTS)
     def _(h):
@@ -362,7 +541,7 @@
 
     @pl.loop(0, CUTS)
     def _(h):
-        total[:, span(h)] = mid_ref[:, span(h)].astype(jnp.float32) + mixed(z, h)
+        total[:, span(h)] += mixed(z, h)
 
         @pl.when(z > 0)
         def _():
@@ -411,45 +590,67 @@
             def _():
                 tab_hop(zs, 1, tabs.at[zs]).wait_send()
 
-
-def routed_by_plane(normed, mid, tab, planes, cap, weights):
-    rows, width = normed.shape
+    for k in range(halves):
+        swap(k, 0).wait_send()
+
+    for side in range(2):
+
+        @pl.when((sp < ends) if side else (sp > 0))
+        def _():
+            halo(side).wait_send()
+
+
+def whole_layer(queries, slab, sinks, gain, routes, shares, out_weight, hidden_in, weights, cap):
+    planes = PLANES
+    rows, width = hidden_in.shape
     tps = lax.axis_size("tp")
     stride = lax.axis_size("sp") // planes
     peers = stride * tps
     slots = peers * cap
+    tok_here, heads_wide = queries.shape
+    bf16, f32 = jnp.bfloat16, jnp.float32
     dma = pltpu.SemaphoreType.DMA
     vmem = pl.BlockSpec(memory_space=pltpu.VMEM)
     anywhere = pl.BlockSpec(memory_space=pl.ANY)
     hidden = weights[0].shape[1]
-    by_slot = pltpu.VMEM((planes, slots, width), jnp.bfloat16)
-    by_row = pltpu.VMEM((planes, rows, width), jnp.bfloat16)
+    by_slot = pltpu.VMEM((planes, slots, width), bf16)
+    by_row = pltpu.VMEM((planes, rows, width), bf16)
     chunks = dma((planes, CUTS))
     fans = dma((planes, CUTS, peers))
+    halves = rows // WIN
     return pl.pallas_call(
         functools.partial(layer_kernel, planes, stride, tps, cap),
-        out_shape=jax.ShapeDtypeStruct((rows, width), jnp.bfloat16),
-        in_specs=[vmem, vmem, vmem, anywhere, anywhere, anywhere],
+        out_shape=jax.ShapeDtypeStruct((rows, width), bf16),
+        in_specs=[vmem, vmem, pl.BlockSpec(memory_space=pltpu.SMEM), vmem, vmem, vmem]
+        + [anywhere] * 5,
         out_specs=vmem,
         scratch_shapes=[
+            pltpu.VMEM((tok_here + 2 * WIN, slab.shape[1]), bf16),
+            pltpu.VMEM((halves + 1, WIN, heads_wide), bf16),
+            pltpu.VMEM((rows, out_weight.shape[0]), bf16),
+            pltpu.VMEM(out_weight.shape, bf16),
+            pltpu.VMEM((rows, width), bf16),
+            pltpu.VMEM((WIN, 3 * WIN), f32),
+            pltpu.VMEM((rows, LANES), f32),
             by_row, by_slot, by_slot, by_slot, by_slot, by_row, by_row, by_row,
-            pltpu.VMEM((width, hidden), jnp.bfloat16),
-            pltpu.VMEM((width, hidden), jnp.bfloat16),
-            pltpu.VMEM((hidden, width), jnp.bfloat16),
-            pltpu.VMEM((slots, hidden), jnp.float32),
-            pltpu.VMEM((slots, hidden), jnp.float32),
-            pltpu.VMEM((slots, hidden), jnp.bfloat16),
-            pltpu.VMEM((planes, rows, slots), jnp.bfloat16),
-            pltpu.VMEM((rows, width), jnp.float32),
-            pltpu.VMEM((planes,) + tab.shape, jnp.float32),
+            pltpu.VMEM((width, hidden), bf16),
+            pltpu.VMEM((width, hidden), bf16),
+            pltpu.VMEM((hidden, width), bf16),
+            pltpu.VMEM((slots, hidden), f32),
+            pltpu.VMEM((slots, hidden), f32),
+            pltpu.VMEM((slots, hidden), bf16),
+            pltpu.VMEM((planes, rows, slots), bf16),
+            pltpu.VMEM((rows, width), f32),
+            pltpu.VMEM((planes, 8, rows), f32),
             dma((2, planes, CUTS)), chunks, fans, fans, fans, fans, chunks, chunks, chunks,
             dma((2, planes)), dma((planes,)), dma((3,)),
+            dma((2,)), dma((2,)), dma((halves,)), dma((halves,)), dma((2,)),
         ],
         compiler_params=pltpu.CompilerParams(
-            collective_id=0, has_side_effects=True, vmem_limit_bytes=60 * 1024 * 1024
+            collective_id=0, has_side_effects=True, vmem_limit_bytes=63 * 1024 * 1024
         ),
-        name="routed",
-    )(normed, tab, mid, *weights)
+        name="layer",
+    )(queries, slab, sinks, gain, routes, shares, out_weight, hidden_in, *weights)
 
 
 def expert_rows(arrived, gate_w, up_w, down_w):
@@ -481,6 +682,36 @@
     kv_here = keys_values.shape[1]
     group = heads_here // kv_here
     head_dim = keys_values.shape[2] // 2
+    topk = routes.shape[1]
+    local_rows, width = hidden_in.shape
+    sp_count = lax.axis_size("sp")
+    tp_count = lax.axis_size("tp")
+    expert_count = sp_count * tp_count
+    capacity = 2 * local_rows * topk // expert_count
+    if (
+        capacity % 16 == 0
+        and sp_count % PLANES == 0
+        and topk == 2
+        and tp_count == 2
+        and 2 * head_dim == LANES
+        and group % 2 == 0
+        and local_rows % WIN == 0
+    ):
+        hot = doc_ids[:, None] == jnp.arange(LANES, dtype=jnp.int32)[None, :]
+        return whole_layer(
+            queries,
+            jnp.concatenate(
+                [keys_values.reshape(tok_here, -1), hot.astype(jnp.bfloat16)], axis=1
+            ),
+            head_sink,
+            norm_gain.reshape(1, width),
+            routes.T,
+            route_weight.T,
+            out_weight,
+            hidden_in,
+            (expert_gate[0], expert_up[0], expert_down[0]),
+            capacity,
+        )
     docs_wide = jnp.broadcast_to(
         doc_ids.astype(jnp.bfloat16)[:, None], (tok_here, keys_values.shape[2])
     )
@@ -541,36 +772,12 @@
         * lax.rsqrt(jnp.mean(mid_wide * mid_wide, axis=-1, keepdims=True) + 1e-06)
         * norm_gain
     ).astype(jnp.bfloat16)
-    local_rows = normed.shape[0]
-    topk = routes.shape[1]
-    width = normed.shape[1]
-    sp_count = lax.axis_size("sp")
-    tp_count = lax.axis_size("tp")
-    expert_count = sp_count * tp_count
-    capacity = 2 * local_rows * topk // expert_count
     flat_routes = routes.reshape(-1)
     one_hot = (flat_routes[:, None] == jnp.arange(expert_count, dtype=jnp.int32)[None, :]).astype(
         jnp.int32
     )
     slot_rank = (jnp.cumsum(one_hot, axis=0) * one_hot).sum(-1) - 1
     slot_index = flat_routes * capacity + slot_rank
-    if capacity % 16 == 0 and sp_count % PLANES == 0 and topk == 2:
-        tab = jnp.concatenate(
-            [
-                slot_index.reshape(local_rows, topk).astype(jnp.float32).T,
-                route_weight.T,
-                jnp.zeros((4, local_rows), jnp.float32),
-            ],
-            axis=0,
-        )
-        return routed_by_plane(
-            normed,
-            mid_wide.astype(jnp.bfloat16),
-            tab,
-            PLANES,
-            capacity,
-            (expert_gate[0], expert_up[0], expert_down[0]),
-        )
     repeated = jnp.repeat(normed, topk, axis=0)
     buffer_rows = (
         jnp.zeros((expert_count * capacity, width), jnp.bfloat16).at[slot_index].set(repeated)

time: 177 us -> 155 us (0.88)
  Pallas kernels: 140 us -> 150 us
  matrix products: 9.69 us -> 0 us
  starting transfers between devices: 6.91 us -> 0 us
  other arithmetic: 8.36 us -> 1.6 us
  waiting for transfers between devices: 4.4 us -> 0 us
  local copies, waits for them, and re-layouts: 7.14 us -> 3.29 us
    pallas_call x1, Pallas kernels: 140 us -> 150 us  [whole_layer(): pl.pallas_call(functools.partial(layer_kernel, planes, stride, tps, cap),...]
    dot_general x3 -> x0, matrix products: 9.69 us -> none  [the longest x1 3.98 us: one_span(): jnp.einsum('hgqk,khd->qhgd', weights, kv_ext[..., head_dim:], preferred_e...]
    ppermute x3 -> x0, starting transfers between devices: 6.91 us -> none  [the longest x1 3.71 us: with_halo(): lax.ppermute(cells[-width:], axis, [(i, (i + 1) % count) for i in range(e...]
    ppermute x3 -> x0, waiting for transfers between devices: 4.4 us -> none  [the longest x1 4.38 us: shards(): lax.ppermute(lax.dynamic_slice_in_dim(attended, (1 - tp) * half, half, 0)...]
    reduce_sum x2 -> x0, other arithmetic: 3.19 us -> none  [the longest x1 3.08 us: one_span(): exp_scores.sum(-1, keepdims=True) + jnp.exp(sink_logit - row_max)]
    unnamed x15 -> x2, local copies, waits for them, and re-layouts: 4.4 us -> 3.29 us
  transfers between devices with their start and end apart: 3 -> 0, of which waited for: 1 -> 0; matrix products, arithmetic and copies ran while one was open for 3% -> 0% of each run, Pallas kernels for 0% -> 0%
where the time goes in v3:
time: 155 us
  Pallas kernels  150 us (97%)
  local copies, waits for them, and re-layouts  3.29 us (2%)
  other arithmetic  1.6 us (1%)
    pallas_call x1, Pallas kernels, whole_layer(): pl.pallas_call(functools.partial(layer_kernel, planes, stride, tps, cap),...  150 us
    unnamed x2, local copies, waits for them, and re-layouts  3.29 us

profile of v3, /device:TPU:9, one launch (start us, length us, event | category | flops | bytes accessed | tf_op | source)
XLA Modules:
  0.0 154.8 jit_solution(12314817610370763527)
XLA Ops:
  0.0 0.8 fusion
  0.8 1.0 copy.15
  1.8 0.8 pad_maximum_fusion.slab_ref
  2.6 149.9 %layer.1 = bf16[256,2048]{1,0:T(8,128)(2,1)} custom-call(bf16[512,512]{1,0:T(8,128)(2,1)} %q_ref.1, bf16[512,384]{1,0:T(8,128)(2,1)} %pad_maximum_fusion.slab_ref, f32[8]{0:T(128)} %sink_ref.1, f32[1,2048]{1,0:T(1,128)} %bitcast.15, s32[2,256]{1,0:T(2,128)} %bitcast.16, f32[2,256]{1,0:T(2,128)} %bitcast.17, bf16[1024,2048]{1,0:T(8,128)(2,1)} %out_w_ref.1, ...), custom_call_target="tpu_custom_call" | custom-call | tf_op jit(solution)/shard_map/layer/pallas_call | solution.py:621
  152.5 2.3 %copy.17 = bf16[256,2048]{1,0:T(8,128)(2,1)} copy(bf16[256,2048]{1,0:T(8,128)(2,1)} %layer.1) | data formatting | bytes 2097152

commit v4 on v3

--- a/solution.py
+++ b/solution.py
@@ -12,6 +12,8 @@
 WIN = 128
 PLANES = 4
 CUTS = 8
+CORES = 2
+TURNS = CUTS // CORES
 TILE = 256
 LAND_LAG = 2
 HELD_LAG = 2
@@ -93,11 +95,11 @@
     planes, stride, tps, cap,
     q_ref, slab_ref, sink_ref, gain_ref, routes_ref, share_ref,
     out_w_ref, hidden_in_ref, gate_ref, up_ref, down_ref, out_ref,
-    reach, outbox, gathered, out_w, resid, bias, squares,
+    reach, outbox, gathered, out_w, resid, bias, squares, lend, lent_mid, leaving, arrived,
     toks, stage, land, results, held, part, from_low, from_high,
     gate_w, up_w, down_w, gate_sum, up_sum, hidden, mixer, total, tabs,
     zsend, zrecv, psend, precv, rsend, rrecv, csend, lowrecv, highrecv, tsend, trecv, wsem,
-    hsend, hrecv, xsend, xrecv, ssem,
+    hsend, hrecv, xsend, xrecv, ssem, lsend, lrecv, msend, mrecv,
 ):
     z, r, tp, p = place(stride, tps)
     peers = stride * tps
@@ -107,6 +109,8 @@
     near = planes - 1
     packed = planes * CUTS
     sp = z * stride + r
+    core = lax.rem(r, CORES)
+    half = width // CORES
     ends = planes * stride - 1
     tok_here, heads_wide = q_ref.shape
     kv_wide = slab_ref.shape[1] - LANES
@@ -179,9 +183,9 @@
     )
     for k in range(2):
         place_in = jnp.sum(chosen[k] * ahead, axis=0, keepdims=True)
-        tabs[z, k : k + 1, :] = picks[k : k + 1, :].astype(jnp.float32) * cap + place_in
-        tabs[z, k + 2 : k + 3, :] = share_ref[k : k + 1, :]
-    tabs[z, 4:8, :] = jnp.zeros((4, rows), jnp.float32)
+        tabs[CORES * z + core, k : k + 1, :] = picks[k : k + 1, :].astype(jnp.float32) * cap + place_in
+        tabs[CORES * z + core, k + 2 : k + 3, :] = share_ref[k : k + 1, :]
+    tabs[CORES * z + core, 4:8, :] = jnp.zeros((4, rows), jnp.float32)
 
     halves = rows // WIN
     span_keys = 3 * WIN
@@ -277,7 +281,8 @@
         mid = resid[:, at].astype(jnp.float32) + jnp.dot(
             gathered[...], out_w[:, at], preferred_element_type=jnp.float32
         )
-        mid = mid.astype(jnp.bfloat16).astype(jnp.float32)
+        resid[:, at] = mid.astype(jnp.bfloat16)
+        mid = resid[:, at].astype(jnp.float32)
         total[:, at] = mid
         square = mid * mid
         for k in range(TILE // LANES):
@@ -297,6 +302,15 @@
     def seat(k):
         return pl.ds(pl.multiple_of(k * cap, cap), cap)
 
+    def wide(side, h):
+        return pl.ds(pl.multiple_of(side * half + h * cols, cols), cols)
+
+    def chip_of(k):
+        return lax.div(k, CORES * tps) * tps + lax.rem(k, tps)
+
+    def core_of(k):
+        return lax.rem(lax.div(k, tps), CORES)
+
     def beside(side):
         return ((z + 1 - 2 * side) * stride + r, tp)
 
@@ -307,16 +321,16 @@
         return pltpu.make_async_remote_copy(
             src_ref=toks.at[zs, :, span(h)],
             dst_ref=toks.at[zs, :, span(h)],
-            send_sem=zsend.at[side, zs, h],
+            send_sem=zsend.at[side, zs],
             recv_sem=zrecv.at[zs, h],
             device_id=beside(side),
             device_id_type=MESH,
         )
 
-    def tab_hop(zs, side, source):
-        return pltpu.make_async_remote_copy(
-            src_ref=source,
-            dst_ref=tabs.at[zs],
+    def tab_hop(zs, side):
+        return pltpu.make_async_remote_copy(
+            src_ref=tabs.at[pl.ds(CORES * zs, CORES)],
+            dst_ref=tabs.at[pl.ds(CORES * zs, CORES)],
             send_sem=tsend.at[side, zs],
             recv_sem=trecv.at[zs],
             device_id=beside(side),
@@ -326,20 +340,62 @@
     def give(zs, h, dest, at):
         return pltpu.make_async_remote_copy(
             src_ref=stage.at[zs, seat(dest), span(h)],
-            dst_ref=land.at[zs, seat(at), span(h)],
-            send_sem=psend.at[zs, h, dest],
-            recv_sem=precv.at[zs, h, at],
+            dst_ref=land.at[zs, seat(chip_of(at)), wide(core_of(at), h)],
+            send_sem=psend.at[zs],
+            recv_sem=precv.at[zs, h],
             device_id=fellow(dest),
             device_id_type=MESH,
         )
 
     def back(zs, h, dest, at):
         return pltpu.make_async_remote_copy(
-            src_ref=results.at[zs, seat(dest), span(h)],
+            src_ref=results.at[zs, seat(chip_of(dest)), wide(core_of(dest), h)],
             dst_ref=held.at[zs, seat(at), span(h)],
-            send_sem=rsend.at[zs, h, dest],
-            recv_sem=rrecv.at[zs, h, at],
+            send_sem=rsend.at[zs],
+            recv_sem=rrecv.at[zs, h],
             device_id=fellow(dest),
+            device_id_type=MESH,
+        )
+
+    def tally(held_by, send_sem, recv_sem):
+        return pltpu.make_async_remote_copy(
+            src_ref=held_by,
+            dst_ref=held_by,
+            send_sem=send_sem,
+            recv_sem=recv_sem,
+            device_id=(sp + 1 - CORES * core, tp),
+            device_id_type=MESH,
+        )
+
+    fan = pl.ds(0, (peers - 1) * cap)
+
+    def to_mate(source, target, which, h):
+        return pltpu.make_async_remote_copy(
+            src_ref=source,
+            dst_ref=target,
+            send_sem=lsend.at[which, h],
+            recv_sem=lrecv.at[which, h],
+            device_id=(sp + 1 - CORES * core, tp),
+            device_id_type=MESH,
+        )
+
+    def lent(h):
+        return to_mate(lend.at[:, span(h)], toks.at[CORES * z + core, :, span(h)], 0, h)
+
+    def lent_rest(h):
+        return to_mate(resid.at[:, wide(1 - core, h)], lent_mid.at[:, span(h)], 1, h)
+
+    def settled(h):
+        return to_mate(leaving.at[:, span(h)], arrived.at[:, span(h)], 2, h)
+
+    def tab_swap():
+        own = tabs.at[CORES * z + core]
+        return pltpu.make_async_remote_copy(
+            src_ref=own,
+            dst_ref=own,
+            send_sem=msend,
+            recv_sem=mrecv,
+            device_id=(sp + 1 - CORES * core, tp),
             device_id_type=MESH,
         )
 
@@ -347,7 +403,7 @@
         return pltpu.make_async_remote_copy(
             src_ref=part.at[zs, :, span(h)],
             dst_ref=from_low.at[zs, :, span(h)],
-            send_sem=csend.at[zs, h],
+            send_sem=csend.at[zs],
             recv_sem=lowrecv.at[zs, h],
             device_id=beside(0),
             device_id_type=MESH,
@@ -357,7 +413,7 @@
         return pltpu.make_async_remote_copy(
             src_ref=part.at[zs, :, span(h)],
             dst_ref=from_high.at[zs, :, span(h)],
-            send_sem=csend.at[zs, h],
+            send_sem=csend.at[zs],
             recv_sem=highrecv.at[zs, h],
             device_id=beside(1),
             device_id_type=MESH,
@@ -370,7 +426,7 @@
         stage[zs, :, span(h)] = picked.astype(jnp.bfloat16)
         for k in range(1, peers):
             give(zs, h, lax.rem(p + k, peers), p).start()
-        land[zs, seat(p), span(h)] = stage[zs, seat(p), span(h)]
+        land[zs, seat(chip_of(p)), wide(core, h)] = stage[zs, seat(p), span(h)]
 
     def expand(zs, h):
         @pl.when(h == 0)
@@ -382,20 +438,21 @@
             gate_sum[...] = jnp.zeros_like(gate_sum)
             up_sum[...] = jnp.zeros_like(up_sum)
 
-        for k in range(1, peers):
-            other = lax.rem(p + k, peers)
-            give(zs, h, other, other).wait_recv()
+        tally(stage.at[zs, fan, span(h)], psend.at[zs], precv.at[zs, h]).wait_recv()
 
         @pl.loop(0, gate_w.shape[1] // TILE)
         def _(c):
             at = pl.ds(pl.multiple_of(c * TILE, TILE), TILE)
-            here = land[zs, :, span(h)]
-            gate_sum[:, at] += jnp.dot(
-                here, gate_w[span(h), at], preferred_element_type=jnp.float32
-            )
-            up_sum[:, at] += jnp.dot(here, up_w[span(h), at], preferred_element_type=jnp.float32)
-
-        @pl.when(h == CUTS - 1)
+            for side in range(CORES):
+                here = land[zs, :, wide(side, h)]
+                gate_sum[:, at] += jnp.dot(
+                    here, gate_w[wide(side, h), at], preferred_element_type=jnp.float32
+                )
+                up_sum[:, at] += jnp.dot(
+                    here, up_w[wide(side, h), at], preferred_element_type=jnp.float32
+                )
+
+        @pl.when(h == TURNS - 1)
         def _():
             @pl.loop(0, gate_w.shape[1] // TILE)
             def _(c):
@@ -406,18 +463,18 @@
                 )
 
     def contract(zs, h):
-        results[zs, :, span(h)] = jnp.dot(
-            hidden[...], down_w[:, span(h)], preferred_element_type=jnp.float32
-        ).astype(jnp.bfloat16)
+        for side in range(CORES):
+            results[zs, :, wide(side, h)] = jnp.dot(
+                hidden[...], down_w[:, wide(side, h)], preferred_element_type=jnp.float32
+            ).astype(jnp.bfloat16)
 
     def send_back(zs, h):
         for k in range(1, peers):
             back(zs, h, lax.rem(p + k, peers), p).start()
-        held[zs, seat(p), span(h)] = results[zs, seat(p), span(h)]
+        held[zs, seat(p), span(h)] = results[zs, seat(chip_of(p)), wide(core, h)]
 
     def mixed(zs, h):
-        for k in range(1, peers):
-            back(zs, h, p, lax.rem(p + k, peers)).wait_recv()
+        tally(stage.at[zs, fan, span(h)], rsend.at[zs], rrecv.at[zs, h]).wait_recv()
         return jnp.dot(mixer[zs], held[zs, :, span(h)], preferred_element_type=jnp.float32)
 
     def homeward(f):
@@ -426,11 +483,12 @@
             down = (k == 0) == (z >= planes // 2)
             g = f - FAR_LAG * k
             round_of = lax.div(g, CUTS) + 1
-            h = lax.rem(g, CUTS)
-            zs = jnp.where(down, near - round_of, round_of)
+            h = lax.rem(g, TURNS)
+            home = jnp.where(down, near - round_of, round_of)
+            zs = CORES * home + lax.rem(lax.div(g, TURNS), CORES)
             due = (g >= 0) & (g < near * CUTS)
 
-            @pl.when(due & down & (zs < z))
+            @pl.when(due & down & (home < z))
             def _():
                 mine = mixed(zs, h)
 
@@ -446,7 +504,7 @@
 
                 sink(zs, h).start()
 
-            @pl.when(due & jnp.logical_not(down) & (zs > z))
+            @pl.when(due & jnp.logical_not(down) & (home > z))
             def _():
                 mine = mixed(zs, h)
 
@@ -462,42 +520,63 @@
 
                 climb(zs, h).start()
 
+    tab_swap().start()
+    for h in range(TURNS):
+        at = wide(1 - core, h)
+        lend[:, span(h)] = (total[:, at] * scale * gain_ref[:, at]).astype(jnp.bfloat16)
+        lent(h).start()
+        lent_rest(h).start()
+
+    @pl.loop(0, TURNS)
+    def _(h):
+        at = wide(core, h)
+        toks[CORES * z + core, :, span(h)] = (total[:, at] * scale * gain_ref[:, at]).astype(
+            jnp.bfloat16
+        )
+
+    tab_swap().wait_recv()
+
     @pl.when(z < near)
     def _():
-        tab_hop(z, 0, tabs.at[z]).start()
+        tab_hop(z, 0).start()
 
     @pl.when(z > 0)
     def _():
-        tab_hop(z, 1, tabs.at[z]).start()
+        tab_hop(z, 1).start()
 
     @pl.loop(0, CUTS)
-    def _(h):
-        at = span(h)
-        toks[z, :, at] = (total[:, at] * scale * gain_ref[:, at]).astype(jnp.bfloat16)
+    def _(k):
+        c = lax.div(k, TURNS)
+        h = lax.rem(k, TURNS)
+
+        @pl.when(c != core)
+        def _():
+            lent(h).wait_recv()
 
         @pl.when(z < near)
         def _():
-            hop(z, h, 0).start()
+            hop(CORES * z + c, h, 0).start()
 
         @pl.when(z > 0)
         def _():
-            hop(z, h, 1).start()
-
-    @pl.loop(0, CUTS)
-    def _(h):
-        pack(z, h)
+            hop(CORES * z + c, h, 1).start()
+
+        pack(CORES * z + c, h)
 
     for load in loads:
         load.wait()
 
     def turn(k):
         nth = lax.div(k, CUTS)
-        return jnp.where(nth < near, block(nth + 1), z), lax.rem(k, CUTS)
-
-    @pl.loop(0, packed + LAND_LAG + CUTS - 1)
+        whose = jnp.where(nth < near, block(nth + 1), z)
+        return CORES * whose + lax.rem(lax.div(k, TURNS), CORES), lax.rem(k, TURNS)
+
+    @pl.loop(0, packed + LAND_LAG + TURNS - 1)
     def _(e):
         dist = lax.div(e, CUTS) + 1
-        h = lax.rem(e, CUTS)
+        i = lax.rem(e, CUTS)
+        c = lax.div(i, TURNS)
+        h = lax.rem(i, TURNS)
 
         @pl.when(dist <= near)
         def _():
@@ -508,21 +587,21 @@
 
                 @pl.when((zs >= 0) & (zs < planes))
                 def _():
-                    @pl.when(h == 0)
+                    @pl.when(i == 0)
                     def _():
-                        tab_hop(zs, side, tabs.at[zs]).wait_recv()
+                        tab_hop(zs, side).wait_recv()
 
                         @pl.when((onward >= 0) & (onward < planes))
                         def _():
-                            tab_hop(zs, side, tabs.at[zs]).start()
-
-                    hop(zs, h, side).wait_recv()
+                            tab_hop(zs, side).start()
+
+                    hop(CORES * zs + c, h, side).wait_recv()
 
                     @pl.when((onward >= 0) & (onward < planes))
                     def _():
-                        hop(zs, h, side).start()
-
-            pack(block(dist), h)
+                        hop(CORES * zs + c, h, side).start()
+
+            pack(CORES * block(dist) + c, h)
 
         g = e - LAND_LAG
 
@@ -530,65 +609,88 @@
         def _():
             expand(*turn(g))
 
-        c = g - CUTS + 1
-
-        @pl.when(c >= 0)
-        def _():
-            contract(*turn(c))
-            send_back(*turn(c))
-
-        homeward(c - HELD_LAG)
+        made = g - TURNS + 1
+
+        @pl.when(made >= 0)
+        def _():
+            contract(*turn(made))
+            send_back(*turn(made))
+
+        homeward(made - HELD_LAG)
+
+    for h in range(TURNS):
+        lent_rest(h).wait_recv()
 
     @pl.loop(0, CUTS)
-    def _(h):
-        total[:, span(h)] += mixed(z, h)
+    def _(k):
+        c = lax.div(k, TURNS)
+        h = lax.rem(k, TURNS)
+        mine = CORES * z + c
+        total[:, span(h)] = mixed(mine, h)
 
         @pl.when(z > 0)
         def _():
-            climb(z, h).wait_recv()
-            total[:, span(h)] += from_low[z, :, span(h)].astype(jnp.float32)
+            climb(mine, h).wait_recv()
+            total[:, span(h)] += from_low[mine, :, span(h)].astype(jnp.float32)
 
         @pl.when(z < near)
         def _():
-            sink(z, h).wait_recv()
-            total[:, span(h)] += from_high[z, :, span(h)].astype(jnp.float32)
-
-        out_ref[:, span(h)] = total[:, span(h)].astype(jnp.bfloat16)
-
-    @pl.loop(0, planes * CUTS)
-    def _(e):
-        zs = lax.div(e, CUTS)
-        h = lax.rem(e, CUTS)
+            sink(mine, h).wait_recv()
+            total[:, span(h)] += from_high[mine, :, span(h)].astype(jnp.float32)
+
+        @pl.when(c == core)
+        def _():
+            at = wide(core, h)
+            out_ref[:, at] = (resid[:, at].astype(jnp.float32) + total[:, span(h)]).astype(
+                jnp.bfloat16
+            )
+
+        @pl.when(c != core)
+        def _():
+            leaving[:, span(h)] = (
+                lent_mid[:, span(h)].astype(jnp.float32) + total[:, span(h)]
+            ).astype(jnp.bfloat16)
+            settled(h).start()
+
+    for h in range(TURNS):
+        settled(h).wait_recv()
+        out_ref[:, wide(1 - core, h)] = arrived[:, span(h)]
+
+    @pl.loop(0, CORES * planes)
+    def _(v):
+        zs = lax.div(v, CORES)
+        sent = toks.at[v]
 
         @pl.when((zs <= z) & (z < near))
         def _():
-            hop(zs, h, 0).wait_send()
+            tally(sent, zsend.at[0, v], zrecv.at[v, 0]).wait_send()
 
         @pl.when((zs >= z) & (z > 0))
         def _():
-            hop(zs, h, 1).wait_send()
-
-        @pl.when(zs > z)
-        def _():
-            climb(zs, h).wait_send()
-
-        @pl.when(zs < z)
-        def _():
-            sink(zs, h).wait_send()
-
-        for k in range(1, peers):
-            give(zs, h, lax.rem(p + k, peers), p).wait_send()
-            back(zs, h, lax.rem(p + k, peers), p).wait_send()
-
-        @pl.when(h == 0)
+            tally(sent, zsend.at[1, v], zrecv.at[v, 0]).wait_send()
+
+        @pl.when(zs != z)
+        def _():
+            tally(sent, csend.at[v], zrecv.at[v, 0]).wait_send()
+
+        tally(stage.at[v, fan, :], psend.at[v], precv.at[v, 0]).wait_send()
+        tally(stage.at[v, fan, :], rsend.at[v], rrecv.at[v, 0]).wait_send()
+
+        @pl.when(lax.rem(v, CORES) == 0)
         def _():
             @pl.when((zs <= z) & (z < near))
             def _():
-                tab_hop(zs, 0, tabs.at[zs]).wait_send()
+                tab_hop(zs, 0).wait_send()
 
             @pl.when((zs >= z) & (z > 0))
             def _():
-                tab_hop(zs, 1, tabs.at[zs]).wait_send()
+                tab_hop(zs, 1).wait_send()
+
+    tab_swap().wait_send()
+    for h in range(TURNS):
+        lent(h).wait_send()
+        lent_rest(h).wait_send()
+        settled(h).wait_send()
 
     for k in range(halves):
         swap(k, 0).wait_send()
@@ -613,10 +715,13 @@
     vmem = pl.BlockSpec(memory_space=pltpu.VMEM)
     anywhere = pl.BlockSpec(memory_space=pl.ANY)
     hidden = weights[0].shape[1]
-    by_slot = pltpu.VMEM((planes, slots, width), bf16)
-    by_row = pltpu.VMEM((planes, rows, width), bf16)
-    chunks = dma((planes, CUTS))
-    fans = dma((planes, CUTS, peers))
+    units = CORES * planes
+    half = width // CORES
+    by_slot = pltpu.VMEM((units, slots, half), bf16)
+    by_chip = pltpu.VMEM((units, slots // CORES, width), bf16)
+    by_row = pltpu.VMEM((units, rows, half), bf16)
+    chunks = dma((units, TURNS))
+    each = dma((units,))
     halves = rows // WIN
     return pl.pallas_call(
         functools.partial(layer_kernel, planes, stride, tps, cap),
@@ -632,19 +737,24 @@
             pltpu.VMEM((rows, width), bf16),
             pltpu.VMEM((WIN, 3 * WIN), f32),
             pltpu.VMEM((rows, LANES), f32),
-            by_row, by_slot, by_slot, by_slot, by_slot, by_row, by_row, by_row,
+            pltpu.VMEM((rows, half), bf16),
+            pltpu.VMEM((rows, half), bf16),
+            pltpu.VMEM((rows, half), bf16),
+            pltpu.VMEM((rows, half), bf16),
+            by_row, by_slot, by_chip, by_chip, by_slot, by_row, by_row, by_row,
             pltpu.VMEM((width, hidden), bf16),
             pltpu.VMEM((width, hidden), bf16),
             pltpu.VMEM((hidden, width), bf16),
-            pltpu.VMEM((slots, hidden), f32),
-            pltpu.VMEM((slots, hidden), f32),
-            pltpu.VMEM((slots, hidden), bf16),
-            pltpu.VMEM((planes, rows, slots), bf16),
+            pltpu.VMEM((slots // CORES, hidden), f32),
+            pltpu.VMEM((slots // CORES, hidden), f32),
+            pltpu.VMEM((slots // CORES, hidden), bf16),
+            pltpu.VMEM((units, rows, slots), bf16),
             pltpu.VMEM((rows, width), f32),
-            pltpu.VMEM((planes, 8, rows), f32),
-            dma((2, planes, CUTS)), chunks, fans, fans, fans, fans, chunks, chunks, chunks,
+            pltpu.VMEM((units, 8, rows), f32),
+            dma((2, units)), chunks, each, chunks, each, chunks, each, chunks, chunks,
             dma((2, planes)), dma((planes,)), dma((3,)),
             dma((2,)), dma((2,)), dma((halves,)), dma((halves,)), dma((2,)),
+            dma((3, TURNS)), dma((3, TURNS)), dma, dma,
         ],
         compiler_params=pltpu.CompilerParams(
             collective_id=0, has_side_effects=True, vmem_limit_bytes=63 * 1024 * 1024
@@ -696,6 +806,7 @@
         and 2 * head_dim == LANES
         and group % 2 == 0
         and local_rows % WIN == 0
+        and sp_count // PLANES % CORES == 0
     ):
         hot = doc_ids[:, None] == jnp.arange(LANES, dtype=jnp.int32)[None, :]
         return whole_layer(

time: 155 us -> 137 us (0.88)
  Pallas kernels: 150 us -> 132 us
    pallas_call x1, Pallas kernels: 150 us -> 132 us  [whole_layer(): pl.pallas_call(functools.partial(layer_kernel, planes, stride, tps, cap),...]
where the time goes in v4:
time: 137 us
  Pallas kernels  132 us (96%)
  local copies, waits for them, and re-layouts  3.29 us (2%)
  other arithmetic  1.6 us (1%)
    pallas_call x1, Pallas kernels, whole_layer(): pl.pallas_call(functools.partial(layer_kernel, planes, stride, tps, cap),...  132 us
    unnamed x2, local copies, waits for them, and re-layouts  3.29 us

profile of v4, /device:TPU:9, one launch (start us, length us, event | category | flops | bytes accessed | tf_op | source)
XLA Modules:
  0.0 136.7 jit_solution(4355046718566662153)
XLA Ops:
  0.0 0.8 fusion
  0.8 1.0 copy.15
  1.8 0.8 pad_maximum_fusion.slab_ref
  2.6 131.8 %layer.1 = bf16[256,2048]{1,0:T(8,128)(2,1)} custom-call(bf16[512,512]{1,0:T(8,128)(2,1)} %q_ref.1, bf16[512,384]{1,0:T(8,128)(2,1)} %pad_maximum_fusion.slab_ref, f32[8]{0:T(128)} %sink_ref.1, f32[1,2048]{1,0:T(1,128)} %bitcast.15, s32[2,256]{1,0:T(2,128)} %bitcast.16, f32[2,256]{1,0:T(2,128)} %bitcast.17, bf16[1024,2048]{1,0:T(8,128)(2,1)} %out_w_ref.1, ...), custom_call_target="tpu_custom_call" | custom-call | tf_op jit(solution)/shard_map/layer/pallas_call | solution.py:726
  134.4 2.3 %copy.17 = bf16[256,2048]{1,0:T(8,128)(2,1)} copy(bf16[256,2048]{1,0:T(8,128)(2,1)} %layer.1) | data formatting | bytes 2097152

commit v5 on v4

--- a/solution.py
+++ b/solution.py
@@ -14,7 +14,7 @@
 CUTS = 8
 CORES = 2
 TURNS = CUTS // CORES
-TILE = 256
+TILE = 512
 LAND_LAG = 2
 HELD_LAG = 2
 FAR_LAG = 2
@@ -82,7 +82,7 @@
     count = peers - 1
     for there in (z > 0, z < planes - 1, first, last):
         count = count + there.astype(jnp.int32)
-    pl.semaphore_wait(barrier, count)
+    return lambda: pl.semaphore_wait(barrier, count)
 
 
 def slot_hits(tab, z, slots, rows):
@@ -93,9 +93,9 @@
 
 def layer_kernel(
     planes, stride, tps, cap,
-    q_ref, slab_ref, sink_ref, gain_ref, routes_ref, share_ref,
+    q_ref, kv_ref, doc_ref, sink_ref, gain_ref, routes_ref, share_ref,
     out_w_ref, hidden_in_ref, gate_ref, up_ref, down_ref, out_ref,
-    reach, outbox, gathered, out_w, resid, bias, squares, lend, lent_mid, leaving, arrived,
+    reach, outbox, gathered, resid, bias, squares, lend, lent_mid, leaving, arrived,
     toks, stage, land, results, held, part, from_low, from_high,
     gate_w, up_w, down_w, gate_sum, up_sum, hidden, mixer, total, tabs,
     zsend, zrecv, psend, precv, rsend, rrecv, csend, lowrecv, highrecv, tsend, trecv, wsem,
@@ -113,11 +113,18 @@
     half = width // CORES
     ends = planes * stride - 1
     tok_here, heads_wide = q_ref.shape
-    kv_wide = slab_ref.shape[1] - LANES
-    starts = [
-        pltpu.make_async_copy(source, target, ssem.at[k])
-        for k, (source, target) in enumerate([(out_w_ref, out_w), (hidden_in_ref, resid)])
-    ]
+    kv_wide = kv_ref.shape[1]
+    deep = out_w_ref.shape[0] // rows
+    starts = [pltpu.make_async_copy(hidden_in_ref, resid, ssem.at[CORES * deep])]
+    for k in range(deep):
+        for side in range(CORES):
+            starts.append(
+                pltpu.make_async_copy(
+                    out_w_ref.at[k * rows : (k + 1) * rows, side * half : (side + 1) * half],
+                    part.at[CORES * k + side],
+                    ssem.at[CORES * k + side],
+                )
+            )
     loads = [
         pltpu.make_async_copy(source, target, wsem.at[k])
         for k, (source, target) in enumerate(
@@ -126,16 +133,27 @@
     ]
     for load in starts:
         load.start()
-    greet(z, r, tp, p, planes, stride, tps)
+    meet = greet(z, r, tp, p, planes, stride, tps)
 
     def halo(side):
         there = 0 if side else tok_here + WIN
         return pltpu.make_async_remote_copy(
-            src_ref=slab_ref.at[pl.ds((tok_here - WIN) * side, WIN), :],
+            src_ref=reach.at[pl.ds(WIN + (tok_here - WIN) * side, WIN), :],
             dst_ref=reach.at[pl.ds(there, WIN), :],
             send_sem=hsend.at[side],
             recv_sem=hrecv.at[side],
             device_id=(sp - 1 + 2 * side, tp),
+            device_id_type=MESH,
+        )
+
+    def tab_swap():
+        own = tabs.at[CORES * z + core]
+        return pltpu.make_async_remote_copy(
+            src_ref=own,
+            dst_ref=own,
+            send_sem=msend,
+            recv_sem=mrecv,
+            device_id=(sp + 1 - CORES * core, tp),
             device_id_type=MESH,
         )
 
@@ -152,12 +170,6 @@
             device_id_type=MESH,
         )
 
-    for side in range(2):
-
-        @pl.when((sp < ends) if side else (sp > 0))
-        def _():
-            halo(side).start()
-
     for load in loads:
         load.start()
 
@@ -169,7 +181,9 @@
     def _():
         reach[tok_here + WIN :, :] = jnp.zeros((WIN, reach.shape[1]), reach.dtype)
 
-    reach[WIN : tok_here + WIN, :] = slab_ref[...]
+    reach[WIN : tok_here + WIN, :kv_wide] = kv_ref[...]
+    document = lax.broadcasted_iota(jnp.int32, (LANES, tok_here), 0) == doc_ref[...]
+    reach[WIN : tok_here + WIN, kv_wide:] = jnp.where(document, 1.0, 0.0).T.astype(jnp.bfloat16)
     picks = routes_ref[...]
     expert = lax.broadcasted_iota(jnp.int32, (planes * peers, rows), 0)
     early = lax.broadcasted_iota(jnp.int32, (rows, rows), 0) < lax.broadcasted_iota(
@@ -243,7 +257,19 @@
             jnp.where(k < halves, halves - 1 - k, k),
         )
 
-    @pl.loop(0, 2 * halves)
+    attend(block_of(0), lambda at: outbox.at[0, :, pl.ds(at, LANES)])
+    meet()
+
+    for side in range(2):
+
+        @pl.when((sp < ends) if side else (sp > 0))
+        def _():
+            halo(side).start()
+
+    swap(0, block_of(0) - halves * (1 - tp)).start()
+    tab_swap().start()
+
+    @pl.loop(1, 2 * halves)
     def _(k):
         b = block_of(k)
 
@@ -272,15 +298,36 @@
     for load in starts:
         load.wait()
     squares[...] = jnp.zeros_like(squares)
+    shared = heads_wide // rows
+
+    def project(side, at, whose):
+        made = 0.0
+        for k in range(shared):
+            row = whose * shared + k
+            made += jnp.dot(
+                gathered[:, pl.ds(pl.multiple_of(row * rows, rows), rows)],
+                part[CORES * row + side, :, at],
+                preferred_element_type=jnp.float32,
+            )
+        return made
+
+    def tile(c):
+        side = lax.div(c * TILE, half)
+        at = pl.ds(pl.multiple_of(c * TILE, TILE), TILE)
+        return side, at, pl.ds(pl.multiple_of(lax.rem(c * TILE, half), TILE), TILE)
+
+    @pl.loop(0, width // TILE)
+    def _(c):
+        side, at, within = tile(c)
+        total[:, at] = resid[:, at].astype(jnp.float32) + project(side, within, tp)
+
     for k in range(halves):
         swap(k, 0).wait_recv()
 
     @pl.loop(0, width // TILE)
     def _(c):
-        at = pl.ds(pl.multiple_of(c * TILE, TILE), TILE)
-        mid = resid[:, at].astype(jnp.float32) + jnp.dot(
-            gathered[...], out_w[:, at], preferred_element_type=jnp.float32
-        )
+        side, at, within = tile(c)
+        mid = total[:, at] + project(side, within, 1 - tp)
         resid[:, at] = mid.astype(jnp.bfloat16)
         mid = resid[:, at].astype(jnp.float32)
         total[:, at] = mid
@@ -387,17 +434,6 @@
 
     def settled(h):
         return to_mate(leaving.at[:, span(h)], arrived.at[:, span(h)], 2, h)
-
-    def tab_swap():
-        own = tabs.at[CORES * z + core]
-        return pltpu.make_async_remote_copy(
-            src_ref=own,
-            dst_ref=own,
-            send_sem=msend,
-            recv_sem=mrecv,
-            device_id=(sp + 1 - CORES * core, tp),
-            device_id_type=MESH,
-        )
 
     def climb(zs, h):
         return pltpu.make_async_remote_copy(
@@ -520,7 +556,6 @@
 
                 climb(zs, h).start()
 
-    tab_swap().start()
     for h in range(TURNS):
         at = wide(1 - core, h)
         lend[:, span(h)] = (total[:, at] * scale * gain_ref[:, at]).astype(jnp.bfloat16)
@@ -702,7 +737,7 @@
             halo(side).wait_send()
 
 
-def whole_layer(queries, slab, sinks, gain, routes, shares, out_weight, hidden_in, weights, cap):
+def whole_layer(queries, kv, docs, sinks, gain, routes, shares, out_weight, hidden_in, weights, cap):
     planes = PLANES
     rows, width = hidden_in.shape
     tps = lax.axis_size("tp")
@@ -725,15 +760,14 @@
     halves = rows // WIN
     return pl.pallas_call(
         functools.partial(layer_kernel, planes, stride, tps, cap),
-        out_shape=jax.ShapeDtypeStruct((rows, width), bf16),
-        in_specs=[vmem, vmem, pl.BlockSpec(memory_space=pltpu.SMEM), vmem, vmem, vmem]
+        out_shape=pltpu.VMEM((rows, width), bf16),
+        in_specs=[vmem, vmem, vmem, pl.BlockSpec(memory_space=pltpu.SMEM), vmem, vmem, vmem]
         + [anywhere] * 5,
         out_specs=vmem,
         scratch_shapes=[
-            pltpu.VMEM((tok_here + 2 * WIN, slab.shape[1]), bf16),
+            pltpu.VMEM((tok_here + 2 * WIN, kv.shape[1] + LANES), bf16),
             pltpu.VMEM((halves + 1, WIN, heads_wide), bf16),
             pltpu.VMEM((rows, out_weight.shape[0]), bf16),
-            pltpu.VMEM(out_weight.shape, bf16),
             pltpu.VMEM((rows, width), bf16),
             pltpu.VMEM((WIN, 3 * WIN), f32),
             pltpu.VMEM((rows, LANES), f32),
@@ -753,14 +787,14 @@
             pltpu.VMEM((units, 8, rows), f32),
             dma((2, units)), chunks, each, chunks, each, chunks, each, chunks, chunks,
             dma((2, planes)), dma((planes,)), dma((3,)),
-            dma((2,)), dma((2,)), dma((halves,)), dma((halves,)), dma((2,)),
+            dma((2,)), dma((2,)), dma((halves,)), dma((halves,)), dma((units + 1,)),
             dma((3, TURNS)), dma((3, TURNS)), dma, dma,
         ],
         compiler_params=pltpu.CompilerParams(
-            collective_id=0, has_side_effects=True, vmem_limit_bytes=63 * 1024 * 1024
+            collective_id=0, has_side_effects=True, vmem_limit_bytes=57 * 1024 * 1024
         ),
         name="layer",
-    )(queries, slab, sinks, gain, routes, shares, out_weight, hidden_in, *weights)
+    )(queries, kv, docs, sinks, gain, routes, shares, out_weight, hidden_in, *weights)
 
 
 def expert_rows(arrived, gate_w, up_w, down_w):
@@ -806,14 +840,15 @@
         and 2 * head_dim == LANES
         and group % 2 == 0
         and local_rows % WIN == 0
+        and local_rows > WIN
+        and out_weight.shape[0] == PLANES * local_rows
+        and queries.shape[1] % local_rows == 0
         and sp_count // PLANES % CORES == 0
     ):
-        hot = doc_ids[:, None] == jnp.arange(LANES, dtype=jnp.int32)[None, :]
         return whole_layer(
             queries,
-            jnp.concatenate(
-                [keys_values.reshape(tok_here, -1), hot.astype(jnp.bfloat16)], axis=1
-            ),
+            keys_values.reshape(tok_here, -1),
+            doc_ids.reshape(1, tok_here),
             head_sink,
             norm_gain.reshape(1, width),
             routes.T,

time: 137 us -> 132 us (0.964)
  Pallas kernels: 132 us -> 129 us
  other arithmetic: 1.6 us -> 0 us
    pallas_call x1, Pallas kernels: 132 us -> 129 us  [whole_layer(): pl.pallas_call(functools.partial(layer_kernel, planes, stride, tps, cap),...]
where the time goes in v5:
time: 132 us
  Pallas kernels  129 us (98%)
  local copies, waits for them, and re-layouts  2.66 us (2%)
    pallas_call x1, Pallas kernels, whole_layer(): pl.pallas_call(functools.partial(layer_kernel, planes, stride, tps, cap),...  129 us
    unnamed x2, local copies, waits for them, and re-layouts  2.66 us

profile of v5, /device:TPU:9, one launch (start us, length us, event | category | flops | bytes accessed | tf_op | source)
XLA Modules:
  0.0 131.6 jit_solution(3903081765761314315)
XLA Ops:
  0.0 1.7 %copy.15 = bf16[64,8,2,128]{3,1,2,0:T(8,128)(2,1)} copy(bf16[64,8,2,128]{3,2,1,0:T(2,128)(2,1)} %bitcast.15) | data formatting | bytes 524288
  1.7 128.9 %layer.1 = bf16[256,2048]{1,0:T(8,128)(2,1)S(1)} custom-call(bf16[512,512]{1,0:T(8,128)(2,1)} %q_ref.1, bf16[512,256]{1,0:T(8,128)(2,1)} %bitcast.14, s32[1,512]{1,0:T(1,128)} %bitcast.17, f32[8]{0:T(128)} %sink_ref.1, f32[1,2048]{1,0:T(1,128)} %bitcast.16, s32[2,256]{1,0:T(2,128)} %bitcast.18, f32[2,256]{1,0:T(2,128)} %bitcast.19, ...), custom_call_target="tpu_custom_call" | custom-call | tf_op jit(solution)/shard_map/layer/pallas_call | solution.py:761
  130.6 1.0 copy.17

commit v6 on v5

--- a/solution.py
+++ b/solution.py
@@ -18,6 +18,7 @@
 LAND_LAG = 2
 HELD_LAG = 2
 FAR_LAG = 2
+LEAD = 3
 MESH = pl.DeviceIdType.MESH
 
 
@@ -338,10 +339,13 @@
     spread = jnp.sum(squares[...], axis=1, keepdims=True) * (1.0 / width)
     scale = lax.rsqrt(spread + 1e-06)
 
+    def far_second(b):
+        return jnp.where(b == 1, 1, jnp.where(b == 2, near, 2))
+
     def block(b):
-        inward = jnp.where(z < planes // 2, z + b, z - b)
-        outward = jnp.where(z < planes // 2, z - 1, z + 1)
-        return jnp.where((inward >= 0) & (inward < planes), inward, outward)
+        at_end = (z == 0) | (z == near)
+        steps = jnp.where(at_end, far_second(b), jnp.where(b == 1, -1, near + 1 - b))
+        return jnp.where(z < planes // 2, z + steps, z - steps)
 
     def span(h):
         return pl.ds(pl.multiple_of(h * cols, cols), cols)
@@ -520,7 +524,8 @@
             g = f - FAR_LAG * k
             round_of = lax.div(g, CUTS) + 1
             h = lax.rem(g, TURNS)
-            home = jnp.where(down, near - round_of, round_of)
+            upper = far_second(round_of)
+            home = jnp.where(down, near - upper, upper)
             zs = CORES * home + lax.rem(lax.div(g, TURNS), CORES)
             due = (g >= 0) & (g < near * CUTS)
 
@@ -588,11 +593,11 @@
         def _():
             lent(h).wait_recv()
 
-        @pl.when(z < near)
+        @pl.when((z < near) & ((z != 1) | (k < LEAD)))
         def _():
             hop(CORES * z + c, h, 0).start()
 
-        @pl.when(z > 0)
+        @pl.when((z > 0) & ((near - z != 1) | (k < LEAD)))
         def _():
             hop(CORES * z + c, h, 1).start()
 
@@ -617,24 +622,45 @@
         def _():
             @pl.loop(0, 2)
             def _(side):
-                zs = z - dist + 2 * dist * side
+                sources = jnp.where(side == 0, z, near - z)
+                second = (e >= LEAD) & (e < LEAD + CUTS)
+                when_two = jnp.where(second, 2, 1)
+                steps = jnp.where(
+                    sources == 1, 1, jnp.where(sources == 2, when_two, far_second(dist))
+                )
+                turn_two = jnp.where(e < LEAD, e, jnp.where(second, e - LEAD, e - CUTS))
+                piece = jnp.where(sources == 2, turn_two, i)
+                zs = z - steps + 2 * steps * side
                 onward = z + 1 - 2 * side
-
-                @pl.when((zs >= 0) & (zs < planes))
+                goes_on = (onward >= 0) & (onward < planes)
+                unit = CORES * zs + lax.div(piece, TURNS)
+                part_of = lax.rem(piece, TURNS)
+
+                @pl.when(e < sources * CUTS)
                 def _():
-                    @pl.when(i == 0)
+                    @pl.when(piece == 0)
                     def _():
                         tab_hop(zs, side).wait_recv()
 
-                        @pl.when((onward >= 0) & (onward < planes))
+                        @pl.when(goes_on)
                         def _():
                             tab_hop(zs, side).start()
 
-                    hop(CORES * zs + c, h, side).wait_recv()
-
-                    @pl.when((onward >= 0) & (onward < planes))
+                    hop(unit, part_of, side).wait_recv()
+
+                    @pl.when(goes_on & (sources == 2) & (e == LEAD + CUTS))
                     def _():
-                        hop(CORES * zs + c, h, side).start()
+                        for k in range(LEAD):
+                            hop(CORES * zs + k // TURNS, k % TURNS, side).start()
+
+                    @pl.when(goes_on & ((sources != 2) | (e >= LEAD)))
+                    def _():
+                        hop(unit, part_of, side).start()
+
+                    @pl.when(goes_on & (sources == 1) & (e == CUTS - 1))
+                    def _():
+                        for k in range(LEAD, CUTS):
+                            hop(CORES * z + k // TURNS, k % TURNS, side).start()
 
             pack(CORES * block(dist) + c, h)
 

time: 132 us -> 129 us (0.977)
  Pallas kernels: 129 us -> 126 us
    pallas_call x1, Pallas kernels: 129 us -> 126 us  [whole_layer(): pl.pallas_call(functools.partial(layer_kernel, planes, stride, tps, cap),...]
where the time goes in v6:
time: 129 us
  Pallas kernels  126 us (98%)
  local copies, waits for them, and re-layouts  2.66 us (2%)
    pallas_call x1, Pallas kernels, whole_layer(): pl.pallas_call(functools.partial(layer_kernel, planes, stride, tps, cap),...  126 us
    unnamed x2, local copies, waits for them, and re-layouts  2.66 us

profile of v6, /device:TPU:9, one launch (start us, length us, event | category | flops | bytes accessed | tf_op | source)
XLA Modules:
  0.0 128.8 jit_solution(9770606717498096552)
XLA Ops:
  0.0 1.7 %copy.15 = bf16[64,8,2,128]{3,1,2,0:T(8,128)(2,1)} copy(bf16[64,8,2,128]{3,2,1,0:T(2,128)(2,1)} %bitcast.15) | data formatting | bytes 524288
  1.7 126.1 %layer.1 = bf16[256,2048]{1,0:T(8,128)(2,1)S(1)} custom-call(bf16[512,512]{1,0:T(8,128)(2,1)} %q_ref.1, bf16[512,256]{1,0:T(8,128)(2,1)} %bitcast.14, s32[1,512]{1,0:T(1,128)} %bitcast.17, f32[8]{0:T(128)} %sink_ref.1, f32[1,2048]{1,0:T(1,128)} %bitcast.16, s32[2,256]{1,0:T(2,128)} %bitcast.18, f32[2,256]{1,0:T(2,128)} %bitcast.19, ...), custom_call_target="tpu_custom_call" | custom-call | tf_op jit(solution)/shard_map/layer/pallas_call | solution.py:787
  127.8 1.0 copy.17
